TPU v7x, 512 devices: a whole 4x4x16 slice. The times are simulated.
512 devices in a mesh: sp: 32 (over z, core), tp: 16 (over y, x).
Axes of the slice: x: 4, y: 4, z: 16, core: 2. Of those that a mesh axis runs over, the one named last changes fastest.
Arguments:
- moe_in: bfloat16 [6144, 2048], P('sp'), may hold values from -6 to 6
- cotangent: bfloat16 [6144, 2048], P('sp'), may hold values from -6 to 6
- routing: int32 [6144, 2], P('sp'), may hold values from 0 to 31, as said below
- route_weight: float32 [6144, 2], P('sp'), may hold values from 0.2 to 1
- w_gate: bfloat16 [32, 2048, 2048], P('sp', 'tp'), may hold values from -0.125 to 0.125
- w_up: bfloat16 [32, 2048, 2048], P('sp', 'tp'), may hold values from -0.125 to 0.125
- w_down: bfloat16 [32, 2048, 2048], P('sp', 'tp'), may hold values from -0.125 to 0.125
- gate_b: bfloat16 [1024, 6144], P('tp', 'sp'), may hold values from -6 to 6
- gate_c: bfloat16 [1024, 6144], P('tp', 'sp'), may hold values from -6 to 6
- value_x: bfloat16 [1024, 6144], P('tp', 'sp'), may hold values from -6 to 6
- conv_taps: float32 [3, 1024], P(None, 'tp'), may hold values from -3 to 3
- out_proj: bfloat16 [1024, 2048], P('tp'), may hold values from -0.1875 to 0.1875
Outputs:
- w_gate_grad: bfloat16 [32, 2048, 2048], P('sp', 'tp')
- w_up_grad: bfloat16 [32, 2048, 2048], P('sp', 'tp')
- w_down_grad: bfloat16 [32, 2048, 2048], P('sp', 'tp')
- moe_in_grad: bfloat16 [6144, 2048], P('sp', 'tp')
- proj_grad: float32 [1024, 2048], P('tp', 'sp')
- gate_b_grad: bfloat16 [1024, 6144], P('tp', 'sp')
- gate_c_grad: bfloat16 [1024, 6144], P('tp', 'sp')
- value_x_grad: bfloat16 [1024, 6144], P('tp', 'sp')
Inputs may be any that keep to these rules, and one draw needn't show every extreme that they name: `routing`: in each aligned block of 192 rows every expert is named exactly 12 times. The two entries of a row are different experts of one group; group g holds experts g * 8 to g * 8 + 7.
All inputs are finite; a program needn't handle non-finite values.
Results may differ from a plain program's by a relative error of at most 0.025.
Values may be sent and summed in bfloat16 or wider, within the bound.
A program may use at most 64 MiB of HBM per device.

v0:
```python
import jax
import jax.numpy as jnp
from jax import lax
from jax.sharding import PartitionSpec as P

TAPS = 3


def side_by_side(arrays, axis, split_dim, concat_dim, along):
    both = jnp.concatenate(arrays, axis=along)
    out, at, done = (
        lax.all_to_all(both, axis, split_axis=split_dim, concat_axis=concat_dim, tiled=True),
        0,
        [],
    )
    for a in arrays:
        done.append(lax.slice_in_dim(out, at, at + a.shape[along], axis=along))
        at += a.shape[along]
    return tuple(done)


def in_one_piece(arrays, axis, dim, along):
    both = jnp.concatenate(arrays, axis=along)
    out, at, done = (lax.all_gather(both, axis, axis=dim, tiled=True), 0, [])
    for a in arrays:
        done.append(lax.slice_in_dim(out, at, at + a.shape[along], axis=along))
        at += a.shape[along]
    return tuple(done)


def cut_along(array, dim, count):
    shape = array.shape
    parts = array.reshape(*shape[:dim], count, shape[dim] // count, *shape[dim + 1 :])
    return jnp.moveaxis(parts, dim, 0)


def sent_and_summed(array, axis, dim):
    parts = cut_along(array, dim, lax.axis_size(axis))
    arrived = lax.all_to_all(parts, axis, split_axis=0, concat_axis=0, tiled=True)
    return arrived.astype(jnp.float32).sum(axis=0)


def sent_to_all(array, axis):
    count = lax.axis_size(axis)
    return lax.all_to_all(
        jnp.broadcast_to(array[None], (count, *array.shape)), axis, 0, 0, tiled=True
    )


def joined_along(parts, dim):
    parts = jnp.moveaxis(parts, 0, dim)
    shape = parts.shape
    return parts.reshape(*shape[:dim], shape[dim] * shape[dim + 1], *shape[dim + 2 :])


def collect(array, axis, dim):
    parts = sent_to_all(array, axis)
    return joined_along(parts, dim)


def from_behind(array, axis, by):
    count = lax.axis_size(axis)
    pairs = [(i, i + by) for i in range(count) if 0 <= i + by < count]
    return lax.ppermute(array, axis, pairs)


def on_device(
    moe_in,
    cotangent,
    routing,
    route_weight,
    w_gate,
    w_up,
    w_down,
    gate_b,
    gate_c,
    value_x,
    conv_taps,
    out_proj,
):
    tok_rows = routing.shape[0]
    top_routes = routing.shape[1]
    experts = lax.axis_size("sp")
    lane_count = lax.axis_size("tp")
    model_width = moe_in.shape[1]
    capacity = top_routes * tok_rows // experts
    flat_routes = routing.reshape(-1)
    route_count = flat_routes.shape[0]
    one_hot = (flat_routes[:, None] == jnp.arange(experts, dtype=jnp.int32)[None, :]).astype(
        jnp.int32
    )
    slot_rank = jnp.sum(jnp.cumsum(one_hot, axis=0) * one_hot, axis=1) - 1
    slot_index = flat_routes * capacity + slot_rank
    source = (
        jnp.zeros((route_count,), jnp.int32)
        .at[slot_index]
        .set(jnp.arange(route_count, dtype=jnp.int32))
    )
    owner_token = source // top_routes
    scales = route_weight.reshape(-1)[source][:, None]
    col_width = model_width // lane_count
    col_start = lax.axis_index("tp") * col_width
    rows_part = lax.dynamic_slice_in_dim(moe_in, col_start, col_width, 1)[owner_token]
    cot_slice = lax.dynamic_slice_in_dim(cotangent, col_start, col_width, 1)[owner_token]
    cot_part = (scales * cot_slice.astype(jnp.float32)).astype(jnp.bfloat16)
    moved = side_by_side((rows_part, cot_part), "sp", 0, 0, 1)
    arrived, arrived_cot = in_one_piece((moved[0], moved[1]), "tp", 1, 0)
    contract_model = (((1,), (1,)), ((), ()))
    over_rows = (((0,), (0,)), ((), ()))
    gate_pre = lax.dot_general(
        arrived, w_gate[0], contract_model, preferred_element_type=jnp.float32
    )
    up_pre = lax.dot_general(arrived, w_up[0], contract_model, preferred_element_type=jnp.float32)
    sigmoid_gate = jax.nn.sigmoid(gate_pre)
    hidden = (gate_pre * sigmoid_gate * up_pre).astype(jnp.bfloat16)
    hidden_grad = lax.dot_general(
        arrived_cot, w_down[0], contract_model, preferred_element_type=jnp.float32
    )
    gate_grad = (
        hidden_grad * up_pre * sigmoid_gate * (1.0 + gate_pre * (1.0 - sigmoid_gate))
    ).astype(jnp.bfloat16)
    up_grad = (hidden_grad * gate_pre * sigmoid_gate).astype(jnp.bfloat16)
    w_gate_grad = lax.dot_general(
        gate_grad, arrived, over_rows, preferred_element_type=jnp.float32
    ).astype(jnp.bfloat16)[None]
    w_up_grad = lax.dot_general(
        up_grad, arrived, over_rows, preferred_element_type=jnp.float32
    ).astype(jnp.bfloat16)[None]
    w_down_grad = lax.dot_general(
        hidden, arrived_cot, over_rows, preferred_element_type=jnp.float32
    ).astype(jnp.bfloat16)[None]
    partial_value = jnp.dot(gate_grad, w_gate[0], preferred_element_type=jnp.float32) + jnp.dot(
        up_grad, w_up[0], preferred_element_type=jnp.float32
    )
    partial_value = lax.optimization_barrier(partial_value.astype(jnp.bfloat16)).astype(jnp.float32)
    summed = sent_and_summed(partial_value.astype(jnp.bfloat16), "tp", 1).astype(jnp.bfloat16)
    returned = lax.all_to_all(summed, "sp", split_axis=0, concat_axis=0, tiled=True)
    per_route = returned[slot_index].astype(jnp.float32)
    moe_in_grad = jnp.sum(per_route.reshape(tok_rows, top_routes, -1), axis=1).astype(jnp.bfloat16)
    full_grad = collect(moe_in_grad, "tp", 1)
    stream_grad = (cotangent.astype(jnp.float32) + full_grad.astype(jnp.float32)).astype(
        jnp.bfloat16
    )
    mixed_in = lax.optimization_barrier(
        (gate_c.astype(jnp.float32) * value_x.astype(jnp.float32)).astype(jnp.bfloat16)
    )
    earlier = from_behind(mixed_in[:, tok_rows - (TAPS - 1) :], "sp", 1)
    extended = jnp.concatenate([earlier, mixed_in], axis=1).astype(jnp.float32)
    conv_out = jnp.zeros(mixed_in.shape, jnp.float32)
    for tap in range(TAPS):
        conv_out = conv_out + conv_taps[tap][:, None] * extended[:, tap : tap + tok_rows]
    mixer_act = (gate_b.astype(jnp.float32) * conv_out).astype(jnp.bfloat16)
    act_grad = lax.dot_general(
        out_proj, stream_grad, contract_model, preferred_element_type=jnp.float32
    )
    proj_rows = sent_and_summed(
        lax.dot_general(
            stream_grad, mixer_act, (((0,), (1,)), ((), ())), preferred_element_type=jnp.float32
        ).astype(jnp.bfloat16),
        "sp",
        0,
    )
    proj_grad = proj_rows.T
    gate_b_grad = (act_grad * conv_out).astype(jnp.bfloat16)
    conv_grad = act_grad * gate_b.astype(jnp.float32)
    later = from_behind(conv_grad[:, : TAPS - 1], "sp", -1)
    extended_grad = jnp.concatenate([conv_grad, later], axis=1)
    mixed_grad = jnp.zeros(conv_grad.shape, jnp.float32)
    for tap in range(TAPS):
        offset = TAPS - 1 - tap
        mixed_grad = (
            mixed_grad + conv_taps[tap][:, None] * extended_grad[:, offset : offset + tok_rows]
        )
    gate_c_grad = (mixed_grad * value_x.astype(jnp.float32)).astype(jnp.bfloat16)
    value_x_grad = (mixed_grad * gate_c.astype(jnp.float32)).astype(jnp.bfloat16)
    return (
        w_gate_grad,
        w_up_grad,
        w_down_grad,
        moe_in_grad,
        proj_grad,
        gate_b_grad,
        gate_c_grad,
        value_x_grad,
    )


def solution(mesh):
    in_specs = (
        P("sp", None),
        P("sp", None),
        P("sp", None),
        P("sp", None),
        P("sp", "tp", None),
        P("sp", "tp", None),
        P("sp", "tp", None),
        P("tp", "sp"),
        P("tp", "sp"),
        P("tp", "sp"),
        P(None, "tp"),
        P("tp", None),
    )
    out_specs = (
        P("sp", "tp", None),
        P("sp", "tp", None),
        P("sp", "tp", None),
        P("sp", "tp"),
        P("tp", "sp"),
        P("tp", "sp"),
        P("tp", "sp"),
        P("tp", "sp"),
    )
    return jax.shard_map(
        on_device, mesh=mesh, in_specs=in_specs, out_specs=out_specs, check_vma=False
    )
```

profile of v0, /device:TPU:1, one launch (start us, length us, event | category | flops | bytes accessed | tf_op | source)
XLA Modules:
  0.0 240.1 jit_solution(9992790808777624512)
XLA Ops:
  7.2 0.0 copy-start
  7.2 0.0 all-gather.2.cloned.1.call-start
  7.2 0.7 broadcast_multiply_fusion
  8.0 0.8 copy.33
  8.8 0.1 eq.25
  8.9 0.1 eq.29
  9.1 0.1 copy.32
  9.2 0.1 mul.126
  9.4 0.9 reduce-window.6
  10.2 0.2 slice_reduce_fusion
  10.5 0.1 fusion.30
  10.6 2.9 %scatter_custom_fusion = s32[384]{0:T(512)S(1)} fusion(s32[384]{0:T(512)S(1)} %fusion.35, s32[384]{0:T(512)S(1)} %iota.11, s32[]{:T(128)} %constant.16.clone.1), kind=kCustom, calls=%fused_computation.87 | custom fusion | bytes 1540 | tf_op jit(solution)/shard_map/scatter | solution.py:97
  13.6 0.8 constant_dynamic-slice_fusion
  14.4 1.4 gather_fusion.2
  15.9 0.1 copy.36
  16.0 0.1 reshape.103
  16.2 2.8 %gather_fusion.1 = f32[384]{0:T(512)S(1)} fusion(f32[384]{0:T(512)S(1)} %reshape.103, s32[1024]{0:T(1024)S(1)} %get-tuple-element.24), kind=kCustom, calls=%fused_computation.1 | custom fusion | bytes 4608 | tf_op jit(solution)/shard_map/gather | solution.py:100
  19.0 0.1 mul.128
  19.1 1.4 gather_fusion
  20.6 0.1 multiply_convert_fusion
  20.8 38.8 %all_to_all.36 = bf16[32,12,256]{2,1,0:T(8,128)(2,1)S(1)} all-to-all(bf16[32,12,256]{2,1,0:T(8,128)(2,1)S(1)} %pad_maximum_fusion), channel_id=1, replica_groups=mesh['sp'=32,'tp'=16] {'sp'}, dimensions={0} | all-to-all | bytes 393216 | tf_op jit(solution)/shard_map/all_to_all | solution.py:12
  59.6 0.7 pad_maximum_fusion.1
  60.3 0.0 all-gather.2.cloned.1.call-update
  60.4 57.2 %all-gather.2.cloned.1.call-done = bf16[768,2048]{1,0:T(8,128)(2,1)} async-done(((bf16[768,128]{1,0:T(8,128)(2,1)}), bf16[768,2048]{1,0:T(8,128)(2,1)}) %all-gather.2.cloned.1.call-update) | async-done | bytes 3145744 | tf_op jit(solution)/shard_map/all_gather | solution.py:24
  117.6 2.1 fusion.9
  119.8 0.0 copy-start.11
  119.8 2.0 fusion.11
  121.8 0.6 multiply_convert_fusion.2
  122.4 0.6 fusion.13
  123.0 0.6 add_convert_fusion
  123.5 0.4 bitcast_bitcast_fusion
  124.0 25.8 %all_to_all.37 = bf16[16,384,128]{2,1,0:T(8,128)(2,1)S(1)} all-to-all(bf16[16,384,128]{2,1,0:T(8,128)(2,1)S(1)} %bitcast_bitcast_fusion), channel_id=1, replica_groups=mesh['sp'=32,'tp'=16] {'tp'}, dimensions={0} | all-to-all | bytes 3145728 | tf_op jit(solution)/shard_map/all_to_all | solution.py:39
  149.7 0.2 reduce_sum.43
  150.0 0.7 all_to_all.26
  150.6 15.5 %all-to-all-start.2 = ((bf16[32,12,128]{2,1,0:T(8,128)(2,1)}), bf16[32,12,128]{2,1,0:T(8,128)(2,1)S(1)}, u32[]{:S(2)}, u32[]{:S(2)}) async-start(bf16[32,12,128]{2,1,0:T(8,128)(2,1)} %all_to_all.26), calls=%async_computation.2 | async-start | bytes 262144 | tf_op jit(solution)/shard_map/all_to_all | solution.py:137
  166.2 15.8 %all-to-all-done.2 = bf16[32,12,128]{2,1,0:T(8,128)(2,1)S(1)} async-done(((bf16[32,12,128]{2,1,0:T(8,128)(2,1)}), bf16[32,12,128]{2,1,0:T(8,128)(2,1)S(1)}, u32[]{:S(2)}, u32[]{:S(2)}) %all-to-all-start.2) | async-done | bytes 98336 | tf_op jit(solution)/shard_map/all_to_all | solution.py:137
  182.1 0.0 copy-start.10
  182.1 1.4 gather_fusion.3
  183.6 0.0 copy-start.12
  183.6 0.2 reduce_sum.44
  183.9 0.0 copy-start.5
  183.9 1.0 broadcast_in_dim.31
  184.9 3.6 %all-to-all-start.3 = ((bf16[16,192,128]{2,1,0:T(8,128)(2,1)}), bf16[16,192,128]{2,1,0:T(8,128)(2,1)S(1)}, u32[]{:S(2)}, u32[]{:S(2)}) async-start(bf16[16,192,128]{2,1,0:T(8,128)(2,1)} %broadcast_in_dim.31), calls=%async_computation.3 | async-start | bytes 1572864 | tf_op jit(solution)/shard_map/all_to_all | solution.py:45
  188.6 0.1 slice.80
  188.6 3.4 %collective-permute-start = (bf16[64,2]{1,0:T(8,128)(2,1)S(1)}, bf16[64,2]{1,0:T(8,128)(2,1)S(1)}, u32[]{:S(2)}, u32[]{:S(2)}) collective-permute-start(bf16[64,2]{1,0:T(8,128)(2,1)S(1)} %slice.80), channel_id=1, source_target_pairs={{0,16},{16,32},{32,48},{48,64},{64,80},{80,96},{96,112},{112,128},... | collective-permute-start | bytes 776 | tf_op jit(solution)/shard_map/ppermute | solution.py:64
  192.1 0.8 collective-permute-done
  192.9 0.1 maximum_convert_fusion
  193.0 8.3 %all-to-all-done.3 = bf16[16,192,128]{2,1,0:T(8,128)(2,1)S(1)} async-done(((bf16[16,192,128]{2,1,0:T(8,128)(2,1)}), bf16[16,192,128]{2,1,0:T(8,128)(2,1)S(1)}, u32[]{:S(2)}, u32[]{:S(2)}) %all-to-all-start.3) | async-done | bytes 786464 | tf_op jit(solution)/shard_map/all_to_all | solution.py:45
  201.2 1.0 multiply_convert_fusion.5
  202.2 0.3 convolution_convert_fusion.3
  202.6 0.5 reshape.105
  203.1 0.2 copy.51
  203.3 1.1 reshape.155
  204.4 6.1 %all-to-all-start.4 = ((bf16[32,2,2048]{2,1,0:T(2,128)(2,1)}), bf16[32,2,2048]{2,1,0:T(2,128)(2,1)S(1)}, u32[]{:S(2)}, u32[]{:S(2)}) async-start(bf16[32,2,2048]{2,1,0:T(2,128)(2,1)} %reshape.155), calls=%async_computation.4 | async-start | bytes 524288 | tf_op jit(solution)/shard_map/all_to_all | solution.py:39
  210.5 2.8 %fusion = bf16[1,128,2048]{2,1,0:T(8,128)(2,1)} fusion(bf16[384,128]{1,0:T(8,128)(2,1)S(1)} %get-tuple-element.13, bf16[768,2048]{1,0:T(8,128)(2,1)} %all-gather.2.cloned.1.call-done), kind=kOutput, calls=%fused_computation.9 | convolution fusion | flops 201588736 | bytes 2195456 | tf_op jit(solution)/shard_map/dot_general | solution.py:123
  213.3 2.7 %fusion.2 = bf16[1,128,2048]{2,1,0:T(8,128)(2,1)} fusion(bf16[768,2048]{1,0:T(8,128)(2,1)} %all-gather.2.cloned.1.call-done, f32[384,128]{1,0:T(8,128)S(1)} %fusion.11, f32[384,128]{1,0:T(8,128)S(1)} %fusion.9), kind=kOutput, calls=%fused_computation.11 | convolution fusion | flops 201883648 | bytes 2490368 | tf_op jit(solution)/shard_map/dot_general | solution.py:129
  216.1 2.3 collective-permute-start.1
  218.3 1.3 fusion.1
  219.6 4.0 %collective-permute-done.1 = f32[64,2]{1,0:T(8,128)S(1)} collective-permute-done((f32[64,2]{1,0:T(8,128)S(1)}, f32[64,2]{1,0:T(8,128)S(1)}, u32[]{:S(2)}, u32[]{:S(2)}) %collective-permute-start.1) | collective-permute-done | bytes 544 | tf_op jit(solution)/shard_map/ppermute | solution.py:64
  223.6 0.8 fusion.21
  224.3 0.6 fusion.23
  225.0 7.2 %all-to-all-done.4 = bf16[32,2,2048]{2,1,0:T(2,128)(2,1)S(1)} async-done(((bf16[32,2,2048]{2,1,0:T(2,128)(2,1)}), bf16[32,2,2048]{2,1,0:T(2,128)(2,1)S(1)}, u32[]{:S(2)}, u32[]{:S(2)}) %all-to-all-start.4) | async-done | bytes 262176 | tf_op jit(solution)/shard_map/all_to_all | solution.py:39
  232.1 0.4 reshape.156
  232.5 0.7 convert_reduce_fusion
  (38 shorter events, 0.3 us)
Async XLA Ops:
  7.2 110.4 %copy-start = (bf16[1,128,2048]{2,1,0:T(8,128)(2,1)S(1)}, bf16[1,128,2048]{2,1,0:T(8,128)(2,1)}, u32[]{:S(2)}) copy-start(bf16[1,128,2048]{2,1,0:T(8,128)(2,1)} %param.16) | copy-start | bytes 1572868
  7.2 8.7 %copy-start.9 = (f32[192,2]{0,1:T(2,128)S(1)}, f32[192,2]{0,1:T(2,128)}, u32[]{:S(2)}) copy-start(f32[192,2]{0,1:T(2,128)} %param.15) | copy-start | bytes 4612
  7.2 110.4 %all-gather.2.cloned.1.call-start = ((), (), s32[]{:S(2)}) async-start(), calls=%async_computation.5 | async-start | bytes 3342336 | tf_op jit(solution)/shard_map/all_gather | solution.py:24
  60.3 59.4 %copy-start.4 = (bf16[1,128,2048]{2,1,0:T(8,128)(2,1)S(1)}, bf16[1,128,2048]{2,1,0:T(8,128)(2,1)}, u32[]{:S(2)}) copy-start(bf16[1,128,2048]{2,1,0:T(8,128)(2,1)} %param.17) | copy-start | bytes 1572868
  117.6 4.2 %copy-start.1 = (bf16[768,2048]{1,0:T(8,128)(2,1)S(1)}, bf16[768,2048]{1,0:T(8,128)(2,1)}, u32[]{:S(2)}) copy-start(bf16[768,2048]{1,0:T(8,128)(2,1)} %all-gather.2.cloned.1.call-done) | copy-start | bytes 9437188
  119.8 2.1 copy-start.11
  150.6 31.4 %all-to-all-start.2 = ((bf16[32,12,128]{2,1,0:T(8,128)(2,1)}), bf16[32,12,128]{2,1,0:T(8,128)(2,1)S(1)}, u32[]{:S(2)}, u32[]{:S(2)}) async-start(bf16[32,12,128]{2,1,0:T(8,128)(2,1)} %all_to_all.26), calls=%async_computation.2 | async-start | bytes 262144 | tf_op jit(solution)/shard_map/all_to_all | solution.py:137
  182.1 6.4 %copy-start.6 = (bf16[64,192]{1,0:T(8,128)(2,1)S(1)}, bf16[64,192]{1,0:T(8,128)(2,1)}, u32[]{:S(2)}) copy-start(bf16[64,192]{1,0:T(8,128)(2,1)} %param.20) | copy-start | bytes 73732
  182.1 6.4 %copy-start.7 = (bf16[64,192]{1,0:T(8,128)(2,1)S(1)}, bf16[64,192]{1,0:T(8,128)(2,1)}, u32[]{:S(2)}) copy-start(bf16[64,192]{1,0:T(8,128)(2,1)} %param.21) | copy-start | bytes 73732
  182.1 9.9 %copy-start.10 = (f32[3,64]{1,0:T(4,128)S(1)}, f32[3,64]{1,0:T(4,128)}, u32[]{:S(2)}) copy-start(f32[3,64]{1,0:T(4,128)} %param.22) | copy-start | bytes 2308
  183.6 17.7 %copy-start.3 = (bf16[192,2048]{1,0:T(8,128)(2,1)S(1)}, bf16[192,2048]{1,0:T(8,128)(2,1)}, u32[]{:S(2)}) copy-start(bf16[192,2048]{1,0:T(8,128)(2,1)} %param.13) | copy-start | bytes 2359300
  183.6 17.7 %copy-start.8 = (bf16[64,192]{1,0:T(8,128)(2,1)S(1)}, bf16[64,192]{1,0:T(8,128)(2,1)}, u32[]{:S(2)}) copy-start(bf16[64,192]{1,0:T(8,128)(2,1)} %param.19) | copy-start | bytes 73732
  183.6 17.6 %copy-start.12 = (bf16[64,2048]{1,0:T(8,128)(2,1)S(1)}, bf16[64,2048]{1,0:T(8,128)(2,1)}, u32[]{:S(2)}) copy-start(bf16[64,2048]{1,0:T(8,128)(2,1)} %param.23) | copy-start | bytes 786436
  183.9 18.4 %copy-start.5 = (bf16[192,128]{1,0:T(8,128)(2,1)}, bf16[192,128]{1,0:T(8,128)(2,1)S(1)}, u32[]{:S(2)}) copy-start(bf16[192,128]{1,0:T(8,128)(2,1)S(1)} %reduce_sum.44) | copy-start | bytes 147460
  184.9 16.3 %all-to-all-start.3 = ((bf16[16,192,128]{2,1,0:T(8,128)(2,1)}), bf16[16,192,128]{2,1,0:T(8,128)(2,1)S(1)}, u32[]{:S(2)}, u32[]{:S(2)}) async-start(bf16[16,192,128]{2,1,0:T(8,128)(2,1)} %broadcast_in_dim.31), calls=%async_computation.3 | async-start | bytes 1572864 | tf_op jit(solution)/shard_map/all_to_all | solution.py:45
  188.6 4.3 %collective-permute-start = (bf16[64,2]{1,0:T(8,128)(2,1)S(1)}, bf16[64,2]{1,0:T(8,128)(2,1)S(1)}, u32[]{:S(2)}, u32[]{:S(2)}) collective-permute-start(bf16[64,2]{1,0:T(8,128)(2,1)S(1)} %slice.80), channel_id=1, source_target_pairs={{0,16},{16,32},{32,48},{48,64},{64,80},{80,96},{96,112},{112,128},... | collective-permute-start | bytes 776 | tf_op jit(solution)/shard_map/ppermute | solution.py:64
  204.4 27.7 %all-to-all-start.4 = ((bf16[32,2,2048]{2,1,0:T(2,128)(2,1)}), bf16[32,2,2048]{2,1,0:T(2,128)(2,1)S(1)}, u32[]{:S(2)}, u32[]{:S(2)}) async-start(bf16[32,2,2048]{2,1,0:T(2,128)(2,1)} %reshape.155), calls=%async_computation.4 | async-start | bytes 524288 | tf_op jit(solution)/shard_map/all_to_all | solution.py:39
  210.5 7.8 %copy-start.2 = (bf16[768,2048]{1,0:T(8,128)(2,1)S(1)}, bf16[768,2048]{1,0:T(8,128)(2,1)}, u32[]{:S(2)}) copy-start(bf16[768,2048]{1,0:T(8,128)(2,1)} %all-gather.2.cloned.1.call-done) | copy-start | bytes 9437188
  216.1 7.5 %collective-permute-start.1 = (f32[64,2]{1,0:T(8,128)S(1)}, f32[64,2]{1,0:T(8,128)S(1)}, u32[]{:S(2)}, u32[]{:S(2)}) collective-permute-start(f32[64,2]{1,0:T(8,128)S(1)} %slice.84), channel_id=1, source_target_pairs={{16,0},{32,16},{48,32},{64,48},{80,64},{96,80},{112,96},{128,112},... | collective-permute-start | bytes 1544 | tf_op jit(solution)/shard_map/ppermute | solution.py:64
Sparse Core Ops, SparseCore 0:
  60.5 57.0 all-gather.1
where the time goes:
time: 241 us; the launch traced here: 240 us
  waiting for transfers between devices  93.3 us (39%)
  blocking collectives  64.6 us (27%)
  starting transfers between devices  30.9 us (13%)
  local copies, waits for them, and re-layouts  17.4 us (7%)
  between operations  14.5 us (6%)
  matrix products  14 us (6%)
  other arithmetic  5.35 us (2%)
    all_gather x1, waiting for transfers between devices, in_one_piece(): out, at, done = (lax.all_gather(both, axis, axis=dim, tiled=True), 0, [])  57.2 us
    all_to_all x1, blocking collectives, side_by_side(): lax.all_to_all(both, axis, split_axis=split_dim, concat_axis=concat_dim,...  38.8 us
    all_to_all x1, blocking collectives, sent_and_summed(): lax.all_to_all(parts, axis, split_axis=0, concat_axis=0, tiled=True)  25.8 us
    all_to_all x1, waiting for transfers between devices, on_device(): lax.all_to_all(summed, 'sp', split_axis=0, concat_axis=0, tiled=True)  15.8 us
    all_to_all x1, starting transfers between devices, on_device(): lax.all_to_all(summed, 'sp', split_axis=0, concat_axis=0, tiled=True)  15.5 us
    all_to_all x1, waiting for transfers between devices, sent_to_all(): lax.all_to_all(jnp.broadcast_to(array[None], (count, *array.shape)), axis...  8.26 us
    all_to_all x1, waiting for transfers between devices, sent_and_summed(): lax.all_to_all(parts, axis, split_axis=0, concat_axis=0, tiled=True)  7.19 us
    all_to_all x1, starting transfers between devices, sent_and_summed(): lax.all_to_all(parts, axis, split_axis=0, concat_axis=0, tiled=True)  6.07 us
  transfers between devices with their start and end apart: 6, of which 6 were waited for; matrix products, arithmetic and copies ran while one was open for 3% of the time, Pallas kernels for 0%

commit v1 on v0

v1 whole, which is shorter than its diff:
```python
import functools

import jax
import jax.numpy as jnp
from jax import lax
from jax.experimental import pallas as pl
from jax.experimental.pallas import tpu as pltpu
from jax.sharding import PartitionSpec as P

MESH = pl.DeviceIdType.MESH
BF = jnp.bfloat16
F32 = jnp.float32
VM = pltpu.VMEM

OFFSETS = (0, 1, -2, 3, -4, 5, -6, 7, -1, 2, -3, 4, -5, 6, -7, 8)
PLACE = {d % 16: j for j, d in enumerate(OFFSETS)}
SLOT = 16
CAP = 12


def nt(a, b):
    return lax.dot_general(a, b, (((1,), (1,)), ((), ())), preferred_element_type=F32)


def nn(a, b):
    return jnp.dot(a, b, preferred_element_type=F32)


def tn(a, b):
    return lax.dot_general(a, b, (((0,), (0,)), ((), ())), preferred_element_type=F32)


def kernel(
    moe_h, cot_h, route_t, weight, wg_h, wu_h, wd_h, gb_h, gc_h, vx_h, taps, op_h,
    o_wg, o_wu, o_wd, o_moe, o_proj, o_gb, o_gc, o_vx,
    moe_v, cot_v, wgu, wdn, gb, gc, vx, op,
    onehot, send, arr, gg, hd, part, r1, r2, zb, t1, t2, fin, ret,
    wgu_o, wdn_o, ggt, hdt, mg, sg,
    mixed, mx_tile, mx_halo, conv, act, cg, cg_tile, cg_halo,
    qb, qp, qs, qr, ts, tp_buf,
    in_sem, out_sem, snd, z1_sem, ag_sem, rs_sem, ret_sem, mg_sem, hl_sem, q_sem,
):
    sp = lax.axis_index("sp")
    tp = lax.axis_index("tp")
    z, core = sp // 2, lax.rem(sp, 2)
    y, x = tp // 4, lax.rem(tp, 4)
    partner = (z * 2 + 1 - core, tp)

    col = pl.ds(pl.multiple_of(tp * 128, 128), 128)
    loads = [
        pltpu.make_async_copy(moe_h.at[:, col], moe_v, in_sem.at[0]),
        pltpu.make_async_copy(cot_h, cot_v, in_sem.at[1]),
        pltpu.make_async_copy(gc_h, gc, in_sem.at[2]),
        pltpu.make_async_copy(vx_h, vx, in_sem.at[3]),
        pltpu.make_async_copy(gb_h, gb, in_sem.at[4]),
        pltpu.make_async_copy(wg_h.at[0], wgu.at[0:128], in_sem.at[5]),
        pltpu.make_async_copy(wu_h.at[0], wgu.at[128:256], in_sem.at[6]),
        pltpu.make_async_copy(wd_h.at[0], wdn, in_sem.at[7]),
        pltpu.make_async_copy(op_h, op, in_sem.at[8]),
    ]
    for c in loads:
        c.start()

    barrier = pltpu.get_barrier_semaphore()
    for b in range(1, 32):
        pl.semaphore_signal(barrier, inc=1, device_id=(lax.rem(sp + b, 32), tp), device_id_type=MESH)

    def near(dim, s):
        if dim == "x":
            return (sp, y * 4 + lax.rem(x + s + 4, 4))
        return (sp, lax.rem(y + s + 4, 4) * 4 + x)

    for dim in ("x", "y"):
        for s in (1, -1):
            pl.semaphore_signal(barrier, inc=1, device_id=near(dim, s), device_id_type=MESH)

    def push(src, dst, group, recv, dev):
        pltpu.make_async_remote_copy(
            src_ref=src, dst_ref=dst, send_sem=snd.at[group], recv_sem=recv, device_id=dev, device_id_type=MESH
        ).start()

    def landed(ref, recv):
        pltpu.make_async_remote_copy(
            src_ref=ref, dst_ref=ref, send_sem=snd.at[0], recv_sem=recv, device_id=partner, device_id_type=MESH
        ).wait_recv()

    def left(ref, group):
        pltpu.make_async_remote_copy(
            src_ref=ref, dst_ref=ref, send_sem=snd.at[group], recv_sem=z1_sem.at[0], device_id=partner,
            device_id_type=MESH,
        ).wait_send()

    def clear(i, carry):
        arr[i, :, :, CAP:SLOT] = jnp.zeros((32, 2, SLOT - CAP, 128), BF)
        return carry

    lax.fori_loop(0, 16, clear, 0)
    ret[:, CAP:SLOT] = jnp.zeros((32, SLOT - CAP, 128), BF)

    expert = lax.broadcasted_iota(jnp.int32, (32, 192), 0)
    first = (route_t[0:1, :] == expert).astype(F32)
    second = (route_t[1:2, :] == expert).astype(F32)
    before = (
        lax.broadcasted_iota(jnp.int32, (192, 192), 0) < lax.broadcasted_iota(jnp.int32, (192, 192), 1)
    ).astype(F32)
    rank = nn((first + second).astype(BF), before.astype(BF))
    spread = (
        (((lax.broadcasted_iota(jnp.int32, (32 * SLOT, 32), 0) >> 4) + sp) & 31)
        == lax.broadcasted_iota(jnp.int32, (32 * SLOT, 32), 1)
    ).astype(F32).astype(BF)
    place = (lax.broadcasted_iota(jnp.int32, (32 * SLOT, 192), 0) & (SLOT - 1)).astype(F32)
    hot0 = (nn(spread, jnp.where(first > 0, rank, -1.0).astype(BF)) == place).astype(F32)
    hot1 = (nn(spread, jnp.where(second > 0, rank, -1.0).astype(BF)) == place).astype(F32)
    onehot[...] = (hot0 + hot1).astype(BF)
    loads[0].wait()
    send[:, 0] = nn(onehot[...], moe_v[...]).astype(BF).reshape(32, SLOT, 128)
    loads[1].wait()
    cot_part = cot_v[:, col].astype(F32)
    cot0 = (weight[:, 0:1] * cot_part).astype(BF)
    cot1 = (weight[:, 1:2] * cot_part).astype(BF)
    routed = nn(hot0.astype(BF), cot0) + nn(hot1.astype(BF), cot1)
    send[:, 1] = routed.astype(BF).reshape(32, SLOT, 128)

    loads[2].wait()
    loads[3].wait()
    mixed[...] = jnp.zeros(mixed.shape, F32)
    mixed[:, 0:192] = (gc[...].astype(F32) * vx[...].astype(F32)).astype(BF).astype(F32)
    mx_tile[...] = pltpu.roll(mixed[:, 128:256], 64, 1).astype(BF)

    arr[tp, core, :, 0:CAP] = send[0, :, 0:CAP]
    pl.semaphore_wait(barrier, 35)

    order = (0, 1, -1, 2, -2, 3, -3, 4, -4, 5, -5, 6, -6, 7, -7, 8)
    for o in order:
        j = PLACE[(-o) % 16]
        zz = lax.rem(z + o + 16, 16)
        for cc in (0, 1):
            e = zz * 2 + cc
            if o == 0:
                if cc == 1:
                    continue
                e = z * 2 + 1 - core
            push(
                send.at[lax.rem(e - sp + 32, 32), :, 0:CAP], arr.at[tp, j * 2 + core, :, 0:CAP], 0,
                z1_sem.at[4 if o == 0 else j // 4], (e, tp),
            )
    after = (lax.rem(sp + 1, 32), tp)
    ahead = (lax.rem(sp + 31, 32), tp)
    push(mx_tile, mx_halo, 1, hl_sem.at[0], after)

    def z_arrived(q):
        a = 8 * q
        if q == 0:
            landed(arr.at[tp, 1 - core, :, 0:CAP], z1_sem.at[4])
            a = 2
        landed(arr.at[tp, a : 8 * q + 8, :, 0:CAP], z1_sem.at[q])

    def gather_steps(region, dims, group, sem):
        d1, d2 = dims

        def lane(a, b):
            dx, dy = (a, b) if d1 == "x" else (b, a)
            return lax.rem(y + dy + 4, 4) * 4 + lax.rem(x + dx + 4, 4)

        def half(s):
            return 0 if s == 1 else 1

        ids = {0: 0, 1: 1, -1: 2, 2: 3}

        def sem1(s):
            return sem(0 if s == 1 else 1)

        def sem2(i, s):
            return sem(3 + ids[i] * 3 + (0 if s == 1 else 1))

        def sem2f(i):
            return sem(3 + ids[i] * 3 + 2)

        def e0():
            own = region(lane(0, 0))
            for s in (1, -1):
                push(own, own, group, sem1(s), near(d1, s))
            for s in (1, -1):
                push(own, own, group, sem2(0, s), near(d2, s))

        def across(i):
            block = region(lane(i, 0))
            for s in (1, -1):
                push(block, block, group, sem2(i, s), near(d2, s))

        def on(i):
            for s in (1, -1):
                landed(region(lane(i, -s)), sem2(i, s))
                block = region(lane(i, -s), half(s))
                push(block, block, group, sem2f(i), near(d2, s))

        def e1():
            for s in (1, -1):
                landed(region(lane(-s, 0)), sem1(s))
                block = region(lane(-s, 0), half(s))
                push(block, block, group, sem(2), near(d1, s))
            for s in (1, -1):
                across(-s)
            on(0)

        def e2():
            landed(region(lane(2, 0)), sem(2))
            across(2)
            on(1)
            on(-1)

        def e3():
            on(2)

        def e4():
            for i in (0, 1, -1, 2):
                landed(region(lane(i, 2)), sem2f(i))

        return e0, e1, e2, e3, e4

    def rows_of(q):
        def region(lane, h=None):
            a, n = (8 * q, 8) if h is None else (8 * q + 4 * h, 4)
            return arr.at[lane, a : a + n, :, 0:CAP]

        return region

    dims_of = (("x", "y"), ("x", "y"), ("y", "x"), ("y", "x"))
    ag = [
        gather_steps(rows_of(q), dims_of[q], 2 + q, functools.partial(lambda q, i: ag_sem.at[q, i], q))
        for q in range(4)
    ]

    def expert_rows(q):
        a = 8 * q
        xm = jnp.concatenate([arr[l, a : a + 8, 0].reshape(128, 128) for l in range(16)], axis=1)
        pre = nt(xm, wgu[...])
        xc = jnp.concatenate([arr[l, a : a + 8, 1].reshape(128, 128) for l in range(16)], axis=1)
        hg = nt(xc, wdn[...])
        gate, up = pre[:, 0:128], pre[:, 128:256]
        sig = jax.nn.sigmoid(gate)
        silu = gate * sig
        rows = slice(128 * q, 128 * q + 128)
        hd[rows, :] = (silu * up).astype(BF)
        gg[rows, 0:128] = (hg * up * sig * (1.0 + gate * (1.0 - sig))).astype(BF)
        gg[rows, 128:256] = (hg * silu).astype(BF)
        g = gg[rows, :]
        for i in range(8):
            pv = nn(g, wgu[:, 256 * i : 256 * i + 256]).astype(BF)
            for k in (0, 1):
                l = 2 * i + k
                part[l // 4, l % 4, a : a + 8] = pv[:, 128 * k : 128 * k + 128].reshape(8, SLOT, 128)

    def back(owner):
        return lax.rem(sp - owner + 32, 32)

    def scatter_steps(q, dims):
        d1, d2 = dims
        at = {"x": x, "y": y}
        a = 8 * q

        def half(s):
            return (0, 4) if s == 1 else (4, 4)

        def bundle(d, lo=0, n=8):
            i = lax.rem(at[d1] + d + 4, 4)
            if d1 == "y":
                return part.at[i, :, a + lo : a + lo + n]
            return part.at[:, i, a + lo : a + lo + n]

        def cut(ref, dims=4):
            return ref.at[:, :, 0:CAP] if dims == 4 else ref.at[:, 0:CAP]

        def w(s):
            return 0 if s == 1 else 1

        def sem(i):
            return rs_sem.at[q, i]

        def q1():
            for s in (1, -1):
                push(cut(bundle(2, *half(s))), cut(r1.at[q, w(s)]), 6 + q, sem(w(s)), near(d1, s))

        def q2():
            for s in (1, -1):
                landed(cut(r1.at[q, w(s)]), sem(w(s)))
                mine = bundle(s, *half(s))
                mine[...] = (mine[...].astype(F32) + r1[q, w(s)].astype(F32)).astype(BF)
                push(cut(bundle(s)), cut(r2.at[q, w(s)]), 6 + q, sem(2 + w(s)), near(d1, s))

        def q3():
            for s in (1, -1):
                landed(cut(r2.at[q, w(s)]), sem(2 + w(s)))
            zb[q] = (bundle(0)[...].astype(F32) + r2[q, 0].astype(F32) + r2[q, 1].astype(F32)).astype(BF)
            i = lax.rem(at[d2] + 2, 4)
            for s in (1, -1):
                lo, n = half(s)
                push(
                    cut(zb.at[q, i, lo : lo + n], 3), cut(t1.at[q, w(s)], 3), 6 + q, sem(4 + w(s)), near(d2, s)
                )

        def q4():
            for s in (1, -1):
                landed(cut(t1.at[q, w(s)], 3), sem(4 + w(s)))
                i = lax.rem(at[d2] + s + 4, 4)
                lo, n = half(s)
                mine = zb.at[q, i, lo : lo + n]
                mine[...] = (mine[...].astype(F32) + t1[q, w(s)].astype(F32)).astype(BF)
                push(cut(zb.at[q, i], 3), cut(t2.at[q, w(s)], 3), 6 + q, sem(6 + w(s)), near(d2, s))

        def q5():
            for s in (1, -1):
                landed(cut(t2.at[q, w(s)], 3), sem(6 + w(s)))
            fin[a : a + 8] = (
                zb[q, at[d2]].astype(F32) + t2[q, 0].astype(F32) + t2[q, 1].astype(F32)
            ).astype(BF)
            for j in range(4 * q, 4 * q + 4):
                for cc in (0, 1):
                    if OFFSETS[j] == 0:
                        if cc == 0:
                            push(fin.at[1 - core, 0:CAP], ret.at[back(partner[0]), 0:CAP], 10, ret_sem, partner)
                            ret[0, 0:CAP] = fin[core, 0:CAP]
                    else:
                        dev = (lax.rem(z + OFFSETS[j] + 16, 16) * 2 + cc, tp)
                        push(fin.at[2 * j + cc, 0:CAP], ret.at[back(dev[0]), 0:CAP], 10, ret_sem, dev)

        return q1, q2, q3, q4, q5

    rs = [scatter_steps(q, dims_of[q][::-1]) for q in range(4)]

    def both(steps, c, k):
        steps[c][k]()
        steps[c + 2][k]()

    z_arrived(0)
    z_arrived(2)
    both(ag, 0, 0)
    both(ag, 0, 1)
    loads[4].wait()
    landed(mx_halo, hl_sem.at[0])
    lane_id = lax.broadcasted_iota(jnp.int32, (64, 128), 1)
    halo = jnp.where(sp == 0, 0.0, mx_halo[...].astype(F32))
    mixed[:, 128:256] = jnp.where(lane_id < 64, mixed[:, 128:256], halo)
    m = mixed[...]
    conv[...] = (
        taps[:, 2:3] * m + taps[:, 1:2] * pltpu.roll(m, 1, 1) + taps[:, 0:1] * pltpu.roll(m, 2, 1)
    )[:, 0:192]
    act[...] = (gb[...].astype(F32) * conv[...]).astype(BF)
    both(ag, 0, 2)
    z_arrived(1)
    z_arrived(3)
    both(ag, 1, 0)
    both(ag, 0, 3)
    both(ag, 1, 1)
    both(ag, 0, 4)
    for c in loads[5:8]:
        c.wait()
    expert_rows(0)
    expert_rows(2)
    both(ag, 1, 2)
    both(rs, 0, 0)
    both(ag, 1, 3)
    both(rs, 0, 1)
    both(ag, 1, 4)
    expert_rows(1)
    expert_rows(3)
    both(rs, 1, 0)
    both(rs, 0, 2)
    both(rs, 1, 1)
    both(rs, 0, 3)

    ggt[...] = gg[...].astype(F32).T.astype(BF)
    hdt[...] = hd[...].astype(F32).T.astype(BF)

    both(rs, 1, 2)
    both(rs, 0, 4)

    def weight_grads(i, carry):
        out = pl.ds(pl.multiple_of(i * 256, 256), 256)
        xm = jnp.concatenate([arr[2 * i, :, 0].reshape(512, 128), arr[2 * i + 1, :, 0].reshape(512, 128)], axis=1)
        wgu_o[:, out] = nn(ggt[...], xm).astype(BF)
        xc = jnp.concatenate([arr[2 * i, :, 1].reshape(512, 128), arr[2 * i + 1, :, 1].reshape(512, 128)], axis=1)
        wdn_o[:, out] = nn(hdt[...], xc).astype(BF)
        return carry

    both(rs, 1, 3)
    both(rs, 1, 4)
    lax.fori_loop(0, 8, weight_grads, 0)
    stores = [
        pltpu.make_async_copy(wgu_o.at[0:128], o_wg.at[0], out_sem.at[0]),
        pltpu.make_async_copy(wgu_o.at[128:256], o_wu.at[0], out_sem.at[1]),
        pltpu.make_async_copy(wdn_o, o_wd.at[0], out_sem.at[2]),
    ]
    for c in stores:
        c.start()

    landed(ret.at[1:32, 0:CAP], ret_sem)
    mine = tn(onehot[...], ret[...].reshape(32 * SLOT, 128)).astype(BF)
    mg[tp] = mine
    o_moe[...] = mine

    def tokens_of(h):
        def region(lane, k=None):
            a, n = (96 * h, 96) if k is None else (96 * h + 48 * k, 48)
            return mg.at[lane, a : a + n]

        return region

    tg = [
        gather_steps(tokens_of(h), (("x", "y"), ("y", "x"))[h], 11 + h, functools.partial(lambda h, i: mg_sem.at[h, i], h))
        for h in range(2)
    ]
    for k in range(5):
        tg[0][k]()
        tg[1][k]()

    for l in range(16):
        lanes = slice(128 * l, 128 * l + 128)
        sg[:, lanes] = (cot_v[:, lanes].astype(F32) + mg[l].astype(F32)).astype(BF)

    for i in range(8):
        pq = nn(act[...], sg[:, 256 * i : 256 * i + 256]).astype(BF)
        for k in (0, 1):
            for h in (0, 1):
                qb[h, 2 * i + k] = pq[32 * h : 32 * h + 32, 128 * k : 128 * k + 128]
    push(qb.at[1 - core], qp, 13, q_sem.at[0], partner)
    loads[8].wait()
    act_grad = nt(op[...], sg[...])
    landed(qp, q_sem.at[0])
    qs[...] = (qb[core].astype(F32) + qp[...].astype(F32)).astype(BF)
    for o in order[:0:-1]:
        zz = lax.rem(z + o + 16, 16)
        push(qs.at[zz], qr.at[PLACE[(-o) % 16]], 14, q_sem.at[1], (zz * 2 + core, tp))

    o_gb[...] = (act_grad * conv[...]).astype(BF)
    cg[...] = jnp.zeros(cg.shape, F32)
    cg[:, 0:192] = act_grad * gb[...].astype(F32)
    cg_tile[...] = pltpu.roll(cg[:, 0:128], 64, 1)
    push(cg_tile, cg_halo, 15, hl_sem.at[1], ahead)
    landed(cg_halo, hl_sem.at[1])
    later = jnp.where(sp == 31, 0.0, cg_halo[...])
    cg[:, 128:256] = jnp.where(lane_id < 64, cg[:, 128:256], later)
    g = cg[...]
    mixed_grad = (
        taps[:, 2:3] * g + taps[:, 1:2] * pltpu.roll(g, 255, 1) + taps[:, 0:1] * pltpu.roll(g, 254, 1)
    )[:, 0:192]
    o_gc[...] = (mixed_grad * vx[...].astype(F32)).astype(BF)
    o_vx[...] = (mixed_grad * gc[...].astype(F32)).astype(BF)

    total = qs[z].astype(F32)
    landed(qr.at[1:16], q_sem.at[1])
    for o in order[1:]:
        total = total + qr[PLACE[o % 16]].astype(F32)
    ts[...] = total
    push(ts, tp_buf, 16, q_sem.at[2], partner)
    landed(tp_buf, q_sem.at[2])
    low = jnp.where(core == 0, ts[...], tp_buf[...])
    high = jnp.where(core == 0, tp_buf[...], ts[...])
    for h, v in ((0, low), (1, high)):
        v = jnp.where(core == 0, v, pltpu.roll(v, 64, 1))
        o_proj[32 * h : 32 * h + 32, :] = v[:, 0:64]

    left(send.at[1:32, :, 0:CAP], 0)
    left(mx_tile, 1)
    for q in range(4):
        left(arr.at[0:15, 8 * q : 8 * q + 8, :, 0:CAP], 2 + q)
        left(arr.at[0:15, 8 * q : 8 * q + 8, 0, 0:CAP], 6 + q)
    left(ret.at[1:32, 0:CAP], 10)
    for h in range(2):
        left(mg.at[0:15, 96 * h : 96 * h + 96], 11 + h)
    left(qp, 13)
    left(qr.at[1:16], 14)
    left(cg_tile, 15)
    left(ts, 16)
    for c in stores:
        c.wait()


def on_device(
    moe_in, cotangent, routing, route_weight, w_gate, w_up, w_down, gate_b, gate_c, value_x, conv_taps, out_proj
):
    hbm = pl.BlockSpec(memory_space=pltpu.HBM)
    vmem = pl.BlockSpec(memory_space=pltpu.VMEM)
    dma = pltpu.SemaphoreType.DMA
    shape = jax.ShapeDtypeStruct
    return pl.pallas_call(
        kernel,
        out_shape=(
            shape(w_gate.shape, BF), shape(w_up.shape, BF), shape(w_down.shape, BF),
            shape((192, 128), BF), shape((64, 64), F32),
            shape((64, 192), BF), shape((64, 192), BF), shape((64, 192), BF),
        ),
        in_specs=[hbm, hbm, vmem, vmem, hbm, hbm, hbm, hbm, hbm, hbm, vmem, hbm],
        out_specs=(hbm, hbm, hbm, vmem, vmem, vmem, vmem, vmem),
        scratch_shapes=[
            VM((192, 128), BF), VM((192, 2048), BF), VM((256, 2048), BF), VM((128, 2048), BF),
            VM((64, 192), BF), VM((64, 192), BF), VM((64, 192), BF), VM((64, 2048), BF),
            VM((512, 192), BF), VM((32, 2, SLOT, 128), BF), VM((16, 32, 2, SLOT, 128), BF),
            VM((512, 256), BF), VM((512, 128), BF), VM((4, 4, 32, SLOT, 128), BF),
            VM((4, 2, 4, 4, SLOT, 128), BF), VM((4, 2, 4, 8, SLOT, 128), BF), VM((4, 4, 8, SLOT, 128), BF),
            VM((4, 2, 4, SLOT, 128), BF), VM((4, 2, 8, SLOT, 128), BF), VM((32, SLOT, 128), BF),
            VM((32, SLOT, 128), BF),
            VM((256, 2048), BF), VM((128, 2048), BF), VM((256, 512), BF), VM((128, 512), BF),
            VM((16, 192, 128), BF), VM((192, 2048), BF),
            VM((64, 256), F32), VM((64, 128), BF), VM((64, 128), BF), VM((64, 192), F32), VM((64, 192), BF),
            VM((64, 256), F32), VM((64, 128), F32), VM((64, 128), F32),
            VM((2, 16, 32, 128), BF), VM((16, 32, 128), BF), VM((16, 32, 128), BF), VM((16, 32, 128), BF),
            VM((32, 128), F32), VM((32, 128), F32),
            dma((9,)), dma((3,)), dma((17,)), dma((5,)), dma((4, 15)), dma((4, 8)), dma, dma((2, 15)), dma((2,)),
            dma((3,)),
        ],
        compiler_params=pltpu.CompilerParams(
            collective_id=0, has_side_effects=True, vmem_limit_bytes=56 * 1024 * 1024
        ),
    )(
        moe_in, cotangent, routing.T, route_weight, w_gate, w_up, w_down, gate_b, gate_c, value_x, conv_taps.T, out_proj
    )


def solution(mesh):
    in_specs = (
        P("sp", None), P("sp", None), P("sp", None), P("sp", None),
        P("sp", "tp", None), P("sp", "tp", None), P("sp", "tp", None),
        P("tp", "sp"), P("tp", "sp"), P("tp", "sp"), P(None, "tp"), P("tp", None),
    )
    out_specs = (
        P("sp", "tp", None), P("sp", "tp", None), P("sp", "tp", None),
        P("sp", "tp"), P("tp", "sp"), P("tp", "sp"), P("tp", "sp"), P("tp", "sp"),
    )
    return jax.shard_map(on_device, mesh=mesh, in_specs=in_specs, out_specs=out_specs, check_vma=False)
```

time: 241 us -> 118 us (0.49)
  Pallas kernels: 0 us -> 107 us
  waiting for transfers between devices: 93.3 us -> 0 us
  blocking collectives: 64.6 us -> 0 us
  starting transfers between devices: 30.9 us -> 0 us
  matrix products: 14 us -> 0 us
  between operations: 14.5 us -> 0.67 us
  local copies, waits for them, and re-layouts: 17.4 us -> 9.81 us
  other arithmetic: 5.35 us -> 0 us
    pallas_call x0 -> x1, Pallas kernels: none -> 107 us  [on_device(): pl.pallas_call(kernel, out_shape=(shape(w_gate.shape, BF), shape(w_up.sha...]
    all_to_all x2 -> x0, blocking collectives: 64.6 us -> none  [the longest x1 38.8 us: side_by_side(): lax.all_to_all(both, axis, split_axis=split_dim, concat_axis=concat_dim,...]
    all_gather x1 -> x0, waiting for transfers between devices: 57.2 us -> none  [in_one_piece(): out, at, done = (lax.all_gather(both, axis, axis=dim, tiled=True), 0, [])]
    all_to_all x3 -> x0, waiting for transfers between devices: 31.3 us -> none  [the longest x1 15.8 us: on_device(): lax.all_to_all(summed, 'sp', split_axis=0, concat_axis=0, tiled=True)]
    all_to_all x3 -> x0, starting transfers between devices: 25.2 us -> none  [the longest x1 15.5 us: on_device(): lax.all_to_all(summed, 'sp', split_axis=0, concat_axis=0, tiled=True)]
    dot_general x10 -> x0, matrix products: 14 us -> none  [the longest x1 2.83 us: on_device(): lax.dot_general(gate_grad, arrived, over_rows, preferred_element_type=jnp...]
    unnamed x30 -> x26, local copies, waits for them, and re-layouts: 2.44 us -> 9.81 us
    gather x4 -> x0, local copies, waits for them, and re-layouts: 7.13 us -> none  [the longest x1 2.8 us: on_device(): scales = route_weight.reshape(-1)[source][:, None]]
  transfers between devices with their start and end apart: 6 -> 0, of which waited for: 6 -> 0; matrix products, arithmetic and copies ran while one was open for 3% -> 0% of each run, Pallas kernels for 0% -> 0%
where the time goes in v1:
time: 118 us; the launch traced here: 117 us
  Pallas kernels  107 us (91%)
  local copies, waits for them, and re-layouts  9.81 us (8%)
    pallas_call x1, Pallas kernels, on_device(): pl.pallas_call(kernel, out_shape=(shape(w_gate.shape, BF), shape(w_up.sha...  107 us
    unnamed x26, local copies, waits for them, and re-layouts  9.81 us

profile of v1, /device:TPU:1, one launch (start us, length us, event | category | flops | bytes accessed | tf_op | source)
XLA Modules:
  0.0 117.2 jit_solution(7265534222662455691)
XLA Ops:
  0.6 0.0 copy-start.7
  0.6 1.4 %copy.20 = f32[3,64]{0,1:T(8,128)} copy(f32[3,64]{1,0:T(4,128)} %param.22) | data formatting | bytes 1536 | tf_op args[10]
  2.0 0.0 copy-done.7
  2.0 0.8 copy.21.weight
  2.8 106.7 %shard_map.179 = (bf16[1,128,2048]{2,1,0:T(8,128)(2,1)}, bf16[1,128,2048]{2,1,0:T(8,128)(2,1)}, bf16[1,128,2048]{2,1,0:T(8,128)(2,1)}, bf16[192,128]{1,0:T(8,128...) custom-call(bf16[192,2048]{1,0:T(8,128)(2,1)} %moe_h.1, ...), custom_call_target="tpu_custom_call" | custom-call | tf_op jit(solution)/shard_map/pallas_call | solution.py:486
  109.6 0.0 copy-start.1
  109.6 1.9 %copy.30 = bf16[1,128,2048]{2,1,0:T(8,128)(2,1)} copy(bf16[1,128,2048]{2,1,0:T(8,128)(2,1)} %get-tuple-element.16) | data formatting | bytes 1048576
  111.5 0.0 copy-done.1
  111.5 0.0 copy-start
  111.5 0.8 copy.31
  112.3 0.4 copy-done
  112.7 0.0 copy-start.2
  112.7 0.8 copy.32
  113.5 0.0 copy-done.2
  113.5 0.0 copy-start.6
  113.5 0.6 copy.33
  114.2 0.1 copy-done.6
  114.3 0.0 copy-start.5
  114.3 0.6 copy.34
  114.9 0.2 copy-done.5
  115.1 0.0 copy-start.4
  115.1 0.6 copy.35
  115.7 0.2 copy-done.4
  115.8 0.0 copy-start.3
  115.8 0.6 copy.36
  116.5 0.2 copy-done.3
  116.6 0.6 copy.37
Async XLA Ops:
  0.6 1.4 %copy-start.7 = (f32[192,2]{0,1:T(2,128)S(1)}, f32[192,2]{0,1:T(2,128)}, u32[]{:S(2)}) copy-start(f32[192,2]{0,1:T(2,128)} %param.15) | copy-start | bytes 4612
  109.6 2.0 %copy-start.1 = (bf16[1,128,2048]{2,1,0:T(8,128)(2,1)S(1)}, bf16[1,128,2048]{2,1,0:T(8,128)(2,1)}, u32[]{:S(2)}) copy-start(bf16[1,128,2048]{2,1,0:T(8,128)(2,1)} %get-tuple-element.17) | copy-start | bytes 1572868
  111.5 1.2 %copy-start = (bf16[1,128,2048]{2,1,0:T(8,128)(2,1)S(1)}, bf16[1,128,2048]{2,1,0:T(8,128)(2,1)}, u32[]{:S(2)}) copy-start(bf16[1,128,2048]{2,1,0:T(8,128)(2,1)} %get-tuple-element.18) | copy-start | bytes 1572868
  112.7 0.8 copy-start.2
  113.5 0.8 copy-start.6
  114.3 0.8 copy-start.5
  115.1 0.8 copy-start.4
  115.8 0.8 copy-start.3

commit v2 on v1

--- a/solution.py
+++ b/solution.py
@@ -31,14 +31,14 @@
 
 
 def kernel(
-    moe_h, cot_h, route_t, weight, wg_h, wu_h, wd_h, gb_h, gc_h, vx_h, taps, op_h,
+    moe_h, cot_h, route_h, weight_h, wg_h, wu_h, wd_h, gb_h, gc_h, vx_h, taps_h, op_h,
     o_wg, o_wu, o_wd, o_moe, o_proj, o_gb, o_gc, o_vx,
-    moe_v, cot_v, wgu, wdn, gb, gc, vx, op,
-    onehot, send, arr, gg, hd, part, r1, r2, zb, t1, t2, fin, ret,
-    wgu_o, wdn_o, ggt, hdt, mg, sg,
+    route_t, weight_v, taps_v, table, turned, moe_v, cot_v, wgu, wdn, gb, gc, vx, op,
+    onehot, send, arr, gg, hd, part, r1, r2, zb, t1, fin, ret,
+    wgu_o, wdn_o, ggt, hdt, mixall, opt, ab, ar, qx,
     mixed, mx_tile, mx_halo, conv, act, cg, cg_tile, cg_halo,
     qb, qp, qs, qr, ts, tp_buf,
-    in_sem, out_sem, snd, z1_sem, ag_sem, rs_sem, ret_sem, mg_sem, hl_sem, q_sem,
+    in_sem, out_sem, snd, z1_sem, ag_sem, rs_sem, ret_sem, w_sem, hl_sem, q_sem,
 ):
     sp = lax.axis_index("sp")
     tp = lax.axis_index("tp")
@@ -46,6 +46,31 @@
     y, x = tp // 4, lax.rem(tp, 4)
     partner = (z * 2 + 1 - core, tp)
 
+    def near(dim, s):
+        if dim == "x":
+            return (sp, y * 4 + lax.rem(x + s + 4, 4))
+        return (sp, lax.rem(y + s + 4, 4) * 4 + x)
+
+    barrier = pltpu.get_barrier_semaphore()
+    order = (0, 1, -1, 2, -2, 3, -3, 4, -4, 5, -5, 6, -6, 7, -7, 8)
+    for o in order[::-1]:
+        zz = lax.rem(z + o + 16, 16)
+        for cc in (0, 1):
+            if o == 0:
+                if cc == 0:
+                    pl.semaphore_signal(barrier, inc=1, device_id=partner, device_id_type=MESH)
+            else:
+                pl.semaphore_signal(barrier, inc=1, device_id=(zz * 2 + cc, tp), device_id_type=MESH)
+    for b in range(1, 16):
+        pl.semaphore_signal(barrier, inc=1, device_id=(sp, lax.rem(tp + b, 16)), device_id_type=MESH)
+
+    small = [
+        pltpu.make_async_copy(route_h, route_t, in_sem.at[9]),
+        pltpu.make_async_copy(weight_h, weight_v, in_sem.at[10]),
+        pltpu.make_async_copy(taps_h, taps_v, in_sem.at[11]),
+    ]
+    for c in small:
+        c.start()
     col = pl.ds(pl.multiple_of(tp * 128, 128), 128)
     loads = [
         pltpu.make_async_copy(moe_h.at[:, col], moe_v, in_sem.at[0]),
@@ -61,19 +86,6 @@
     for c in loads:
         c.start()
 
-    barrier = pltpu.get_barrier_semaphore()
-    for b in range(1, 32):
-        pl.semaphore_signal(barrier, inc=1, device_id=(lax.rem(sp + b, 32), tp), device_id_type=MESH)
-
-    def near(dim, s):
-        if dim == "x":
-            return (sp, y * 4 + lax.rem(x + s + 4, 4))
-        return (sp, lax.rem(y + s + 4, 4) * 4 + x)
-
-    for dim in ("x", "y"):
-        for s in (1, -1):
-            pl.semaphore_signal(barrier, inc=1, device_id=near(dim, s), device_id_type=MESH)
-
     def push(src, dst, group, recv, dev):
         pltpu.make_async_remote_copy(
             src_ref=src, dst_ref=dst, send_sem=snd.at[group], recv_sem=recv, device_id=dev, device_id_type=MESH
@@ -96,6 +108,14 @@
 
     lax.fori_loop(0, 16, clear, 0)
     ret[:, CAP:SLOT] = jnp.zeros((32, SLOT - CAP, 128), BF)
+
+    table[...] = jnp.zeros(table.shape, F32)
+    for c in small:
+        c.wait()
+    table[0:2, 0:192] = weight_v[...]
+    table[8:11, 0:64] = taps_v[...]
+    turned[...] = table[...].T
+    taps = [turned[0:64, 8 + j : 9 + j] for j in range(3)]
 
     expert = lax.broadcasted_iota(jnp.int32, (32, 192), 0)
     first = (route_t[0:1, :] == expert).astype(F32)
@@ -116,8 +136,8 @@
     send[:, 0] = nn(onehot[...], moe_v[...]).astype(BF).reshape(32, SLOT, 128)
     loads[1].wait()
     cot_part = cot_v[:, col].astype(F32)
-    cot0 = (weight[:, 0:1] * cot_part).astype(BF)
-    cot1 = (weight[:, 1:2] * cot_part).astype(BF)
+    cot0 = (turned[0:192, 0:1] * cot_part).astype(BF)
+    cot1 = (turned[0:192, 1:2] * cot_part).astype(BF)
     routed = nn(hot0.astype(BF), cot0) + nn(hot1.astype(BF), cot1)
     send[:, 1] = routed.astype(BF).reshape(32, SLOT, 128)
 
@@ -128,10 +148,9 @@
     mx_tile[...] = pltpu.roll(mixed[:, 128:256], 64, 1).astype(BF)
 
     arr[tp, core, :, 0:CAP] = send[0, :, 0:CAP]
-    pl.semaphore_wait(barrier, 35)
-
-    order = (0, 1, -1, 2, -2, 3, -3, 4, -4, 5, -5, 6, -6, 7, -7, 8)
-    for o in order:
+    pl.semaphore_wait(barrier, 46)
+
+    def dispatch_to(o):
         j = PLACE[(-o) % 16]
         zz = lax.rem(z + o + 16, 16)
         for cc in (0, 1):
@@ -142,18 +161,21 @@
                 e = z * 2 + 1 - core
             push(
                 send.at[lax.rem(e - sp + 32, 32), :, 0:CAP], arr.at[tp, j * 2 + core, :, 0:CAP], 0,
-                z1_sem.at[4 if o == 0 else j // 4], (e, tp),
+                z1_sem.at[8 if o == 0 else j // 2], (e, tp),
             )
+
+    for o in order:
+        dispatch_to(o)
     after = (lax.rem(sp + 1, 32), tp)
     ahead = (lax.rem(sp + 31, 32), tp)
     push(mx_tile, mx_halo, 1, hl_sem.at[0], after)
 
-    def z_arrived(q):
-        a = 8 * q
-        if q == 0:
-            landed(arr.at[tp, 1 - core, :, 0:CAP], z1_sem.at[4])
+    def z_arrived(i):
+        a = 4 * i
+        if i == 0:
+            landed(arr.at[tp, 1 - core, :, 0:CAP], z1_sem.at[8])
             a = 2
-        landed(arr.at[tp, a : 8 * q + 8, :, 0:CAP], z1_sem.at[q])
+        landed(arr.at[tp, a : 4 * i + 4, :, 0:CAP], z1_sem.at[i])
 
     def gather_steps(region, dims, group, sem):
         d1, d2 = dims
@@ -220,15 +242,15 @@
 
     def rows_of(q):
         def region(lane, h=None):
-            a, n = (8 * q, 8) if h is None else (8 * q + 4 * h, 4)
+            a, n = (4 * q, 4) if h is None else (4 * q + 2 * h, 2)
             return arr.at[lane, a : a + n, :, 0:CAP]
 
         return region
 
     dims_of = (("x", "y"), ("x", "y"), ("y", "x"), ("y", "x"))
     ag = [
-        gather_steps(rows_of(q), dims_of[q], 2 + q, functools.partial(lambda q, i: ag_sem.at[q, i], q))
-        for q in range(4)
+        gather_steps(rows_of(i), dims_of[i // 2], 2 + i, functools.partial(lambda i, k: ag_sem.at[i, k], i))
+        for i in range(8)
     ]
 
     def expert_rows(q):
@@ -279,63 +301,57 @@
 
         def q1():
             for s in (1, -1):
-                push(cut(bundle(2, *half(s))), cut(r1.at[q, w(s)]), 6 + q, sem(w(s)), near(d1, s))
+                push(cut(bundle(2, *half(s))), cut(r1.at[q, w(s)]), 10 + q, sem(w(s)), near(d1, s))
 
         def q2():
             for s in (1, -1):
                 landed(cut(r1.at[q, w(s)]), sem(w(s)))
                 mine = bundle(s, *half(s))
                 mine[...] = (mine[...].astype(F32) + r1[q, w(s)].astype(F32)).astype(BF)
-                push(cut(bundle(s)), cut(r2.at[q, w(s)]), 6 + q, sem(2 + w(s)), near(d1, s))
+                push(cut(bundle(s)), cut(r2.at[q, w(s)]), 10 + q, sem(2 + w(s)), near(d1, s))
 
         def q3():
             for s in (1, -1):
                 landed(cut(r2.at[q, w(s)]), sem(2 + w(s)))
             zb[q] = (bundle(0)[...].astype(F32) + r2[q, 0].astype(F32) + r2[q, 1].astype(F32)).astype(BF)
-            i = lax.rem(at[d2] + 2, 4)
-            for s in (1, -1):
-                lo, n = half(s)
-                push(
-                    cut(zb.at[q, i, lo : lo + n], 3), cut(t1.at[q, w(s)], 3), 6 + q, sem(4 + w(s)), near(d2, s)
-                )
+            for k, s in enumerate((2, 1, -1)):
+                i = lax.rem(at[d2] + s + 4, 4)
+                push(cut(zb.at[q, i], 3), cut(t1.at[q, k], 3), 10 + q, sem(4 + k), near(d2, s))
 
         def q4():
-            for s in (1, -1):
-                landed(cut(t1.at[q, w(s)], 3), sem(4 + w(s)))
-                i = lax.rem(at[d2] + s + 4, 4)
-                lo, n = half(s)
-                mine = zb.at[q, i, lo : lo + n]
-                mine[...] = (mine[...].astype(F32) + t1[q, w(s)].astype(F32)).astype(BF)
-                push(cut(zb.at[q, i], 3), cut(t2.at[q, w(s)], 3), 6 + q, sem(6 + w(s)), near(d2, s))
-
-        def q5():
-            for s in (1, -1):
-                landed(cut(t2.at[q, w(s)], 3), sem(6 + w(s)))
+            for k in range(3):
+                landed(cut(t1.at[q, k], 3), sem(4 + k))
             fin[a : a + 8] = (
-                zb[q, at[d2]].astype(F32) + t2[q, 0].astype(F32) + t2[q, 1].astype(F32)
+                zb[q, at[d2]].astype(F32) + t1[q, 0].astype(F32) + t1[q, 1].astype(F32) + t1[q, 2].astype(F32)
             ).astype(BF)
-            for j in range(4 * q, 4 * q + 4):
+            for j in range(4 * q + 3, 4 * q - 1, -1):
                 for cc in (0, 1):
                     if OFFSETS[j] == 0:
                         if cc == 0:
-                            push(fin.at[1 - core, 0:CAP], ret.at[back(partner[0]), 0:CAP], 10, ret_sem, partner)
+                            push(fin.at[1 - core, 0:CAP], ret.at[back(partner[0]), 0:CAP], 14, ret_sem, partner)
                             ret[0, 0:CAP] = fin[core, 0:CAP]
                     else:
                         dev = (lax.rem(z + OFFSETS[j] + 16, 16) * 2 + cc, tp)
-                        push(fin.at[2 * j + cc, 0:CAP], ret.at[back(dev[0]), 0:CAP], 10, ret_sem, dev)
-
-        return q1, q2, q3, q4, q5
+                        push(fin.at[2 * j + cc, 0:CAP], ret.at[back(dev[0]), 0:CAP], 14, ret_sem, dev)
+
+        return q1, q2, q3, q4
 
     rs = [scatter_steps(q, dims_of[q][::-1]) for q in range(4)]
 
     def both(steps, c, k):
         steps[c][k]()
-        steps[c + 2][k]()
+        steps[c + len(steps) // 2][k]()
 
     z_arrived(0)
+    z_arrived(4)
+    both(ag, 0, 0)
+    z_arrived(1)
+    z_arrived(5)
+    both(ag, 1, 0)
+    both(ag, 0, 1)
     z_arrived(2)
-    both(ag, 0, 0)
-    both(ag, 0, 1)
+    z_arrived(6)
+    both(ag, 2, 0)
     loads[4].wait()
     landed(mx_halo, hl_sem.at[0])
     lane_id = lax.broadcasted_iota(jnp.int32, (64, 128), 1)
@@ -343,37 +359,43 @@
     mixed[:, 128:256] = jnp.where(lane_id < 64, mixed[:, 128:256], halo)
     m = mixed[...]
     conv[...] = (
-        taps[:, 2:3] * m + taps[:, 1:2] * pltpu.roll(m, 1, 1) + taps[:, 0:1] * pltpu.roll(m, 2, 1)
+        taps[2] * m + taps[1] * pltpu.roll(m, 1, 1) + taps[0] * pltpu.roll(m, 2, 1)
     )[:, 0:192]
     act[...] = (gb[...].astype(F32) * conv[...]).astype(BF)
+    for c in loads[5:9]:
+        c.wait()
+    both(ag, 1, 1)
+    z_arrived(3)
+    z_arrived(7)
+    both(ag, 3, 0)
     both(ag, 0, 2)
-    z_arrived(1)
-    z_arrived(3)
-    both(ag, 1, 0)
+    both(ag, 2, 1)
+    both(ag, 1, 2)
+    both(ag, 3, 1)
     both(ag, 0, 3)
-    both(ag, 1, 1)
+    both(ag, 2, 2)
+    both(ag, 1, 3)
     both(ag, 0, 4)
-    for c in loads[5:8]:
-        c.wait()
+    both(ag, 3, 2)
+    both(ag, 2, 3)
+    both(ag, 1, 4)
+    both(ag, 3, 3)
     expert_rows(0)
     expert_rows(2)
-    both(ag, 1, 2)
     both(rs, 0, 0)
-    both(ag, 1, 3)
-    both(rs, 0, 1)
-    both(ag, 1, 4)
+    both(ag, 2, 4)
+    both(ag, 3, 4)
     expert_rows(1)
     expert_rows(3)
     both(rs, 1, 0)
+    both(rs, 0, 1)
+    both(rs, 1, 1)
     both(rs, 0, 2)
-    both(rs, 1, 1)
+    both(rs, 1, 2)
     both(rs, 0, 3)
 
     ggt[...] = gg[...].astype(F32).T.astype(BF)
     hdt[...] = hd[...].astype(F32).T.astype(BF)
-
-    both(rs, 1, 2)
-    both(rs, 0, 4)
 
     def weight_grads(i, carry):
         out = pl.ds(pl.multiple_of(i * 256, 256), 256)
@@ -384,7 +406,16 @@
         return carry
 
     both(rs, 1, 3)
-    both(rs, 1, 4)
+
+    mixall[0] = act[...]
+    opt[0] = op[:, col]
+    for b in range(1, 16):
+        lane = lax.rem(tp + b, 16)
+        push(act, mixall.at[16 - b], 15, w_sem.at[0], (sp, lane))
+    for b in range(1, 16):
+        lane = lax.rem(tp + b, 16)
+        there = pl.ds(pl.multiple_of(lane * 128, 128), 128)
+        push(op.at[:, there], opt.at[16 - b], 16, w_sem.at[1], (sp, lane))
     lax.fori_loop(0, 8, weight_grads, 0)
     stores = [
         pltpu.make_async_copy(wgu_o.at[0:128], o_wg.at[0], out_sem.at[0]),
@@ -396,63 +427,58 @@
 
     landed(ret.at[1:32, 0:CAP], ret_sem)
     mine = tn(onehot[...], ret[...].reshape(32 * SLOT, 128)).astype(BF)
-    mg[tp] = mine
     o_moe[...] = mine
-
-    def tokens_of(h):
-        def region(lane, k=None):
-            a, n = (96 * h, 96) if k is None else (96 * h + 48 * k, 48)
-            return mg.at[lane, a : a + n]
-
-        return region
-
-    tg = [
-        gather_steps(tokens_of(h), (("x", "y"), ("y", "x"))[h], 11 + h, functools.partial(lambda h, i: mg_sem.at[h, i], h))
-        for h in range(2)
-    ]
-    for k in range(5):
-        tg[0][k]()
-        tg[1][k]()
-
-    for l in range(16):
-        lanes = slice(128 * l, 128 * l + 128)
-        sg[:, lanes] = (cot_v[:, lanes].astype(F32) + mg[l].astype(F32)).astype(BF)
-
-    for i in range(8):
-        pq = nn(act[...], sg[:, 256 * i : 256 * i + 256]).astype(BF)
-        for k in (0, 1):
-            for h in (0, 1):
-                qb[h, 2 * i + k] = pq[32 * h : 32 * h + 32, 128 * k : 128 * k + 128]
-    push(qb.at[1 - core], qp, 13, q_sem.at[0], partner)
-    loads[8].wait()
-    act_grad = nt(op[...], sg[...])
+    stream = (cot_v[:, col].astype(F32) + mine.astype(F32)).astype(BF)
+
+    landed(mixall.at[1:16], w_sem.at[0])
+    for i in range(4):
+        pq = nn(mixall[4 * i : 4 * i + 4].reshape(256, 192), stream).astype(BF).reshape(4, 2, 32, 128)
+        for h in (0, 1):
+            qb[h, 4 * i : 4 * i + 4] = pq[:, h]
+    push(qb.at[1 - core], qp, 17, q_sem.at[0], partner)
+    landed(opt.at[1:16], w_sem.at[1])
+    for i in range(4):
+        pa = nt(opt[4 * i : 4 * i + 4].reshape(256, 128), stream).astype(BF)
+        ab[4 * i : 4 * i + 4] = pa.reshape(4, 64, 192)
     landed(qp, q_sem.at[0])
     qs[...] = (qb[core].astype(F32) + qp[...].astype(F32)).astype(BF)
+    qx[0] = qs[0]
+    for b in range(1, 16):
+        push(qs.at[b], qx.at[16 - b], 18, q_sem.at[3], (sp, lax.rem(tp + b, 16)))
+    for b in range(1, 16):
+        push(ab.at[b], ar.at[16 - b], 19, w_sem.at[2], (sp, lax.rem(tp + b, 16)))
+    landed(qx.at[1:16], q_sem.at[3])
     for o in order[:0:-1]:
         zz = lax.rem(z + o + 16, 16)
-        push(qs.at[zz], qr.at[PLACE[(-o) % 16]], 14, q_sem.at[1], (zz * 2 + core, tp))
+        push(
+            qx.at[lax.rem(zz - tp + 16, 16)], qr.at[PLACE[(-o) % 16]], 20, q_sem.at[1], (zz * 2 + core, tp)
+        )
+    landed(ar.at[1:16], w_sem.at[2])
+    act_grad = ab[0].astype(F32)
+    for b in range(1, 16):
+        act_grad = act_grad + ar[b].astype(F32)
 
     o_gb[...] = (act_grad * conv[...]).astype(BF)
     cg[...] = jnp.zeros(cg.shape, F32)
     cg[:, 0:192] = act_grad * gb[...].astype(F32)
     cg_tile[...] = pltpu.roll(cg[:, 0:128], 64, 1)
-    push(cg_tile, cg_halo, 15, hl_sem.at[1], ahead)
+    push(cg_tile, cg_halo, 21, hl_sem.at[1], ahead)
     landed(cg_halo, hl_sem.at[1])
     later = jnp.where(sp == 31, 0.0, cg_halo[...])
     cg[:, 128:256] = jnp.where(lane_id < 64, cg[:, 128:256], later)
     g = cg[...]
     mixed_grad = (
-        taps[:, 2:3] * g + taps[:, 1:2] * pltpu.roll(g, 255, 1) + taps[:, 0:1] * pltpu.roll(g, 254, 1)
+        taps[2] * g + taps[1] * pltpu.roll(g, 255, 1) + taps[0] * pltpu.roll(g, 254, 1)
     )[:, 0:192]
     o_gc[...] = (mixed_grad * vx[...].astype(F32)).astype(BF)
     o_vx[...] = (mixed_grad * gc[...].astype(F32)).astype(BF)
 
-    total = qs[z].astype(F32)
+    total = qx[lax.rem(z - tp + 16, 16)].astype(F32)
     landed(qr.at[1:16], q_sem.at[1])
     for o in order[1:]:
         total = total + qr[PLACE[o % 16]].astype(F32)
     ts[...] = total
-    push(ts, tp_buf, 16, q_sem.at[2], partner)
+    push(ts, tp_buf, 22, q_sem.at[2], partner)
     landed(tp_buf, q_sem.at[2])
     low = jnp.where(core == 0, ts[...], tp_buf[...])
     high = jnp.where(core == 0, tp_buf[...], ts[...])
@@ -462,18 +488,47 @@
 
     left(send.at[1:32, :, 0:CAP], 0)
     left(mx_tile, 1)
+    for i in range(8):
+        left(arr.at[0:15, 4 * i : 4 * i + 4, :, 0:CAP], 2 + i)
     for q in range(4):
-        left(arr.at[0:15, 8 * q : 8 * q + 8, :, 0:CAP], 2 + q)
-        left(arr.at[0:15, 8 * q : 8 * q + 8, 0, 0:CAP], 6 + q)
-    left(ret.at[1:32, 0:CAP], 10)
-    for h in range(2):
-        left(mg.at[0:15, 96 * h : 96 * h + 96], 11 + h)
-    left(qp, 13)
-    left(qr.at[1:16], 14)
-    left(cg_tile, 15)
-    left(ts, 16)
+        left(arr.at[0:15, 8 * q : 8 * q + 8, 0, 0:CAP], 10 + q)
+    left(ret.at[1:32, 0:CAP], 14)
+    left(mixall.at[1:16], 15)
+    left(opt.at[1:16], 16)
+    left(qp, 17)
+    left(qx.at[1:16], 18)
+    left(ar.at[1:16], 19)
+    left(qr.at[1:16], 20)
+    left(cg_tile, 21)
+    left(ts, 22)
     for c in stores:
         c.wait()
+
+
+def copy_kernel(*refs):
+    ins, outs, rest = refs[:8], refs[8:16], refs[16:]
+    bufs, sem_in, sem_out = rest[:8], rest[8], rest[9]
+    reads = [pltpu.make_async_copy(a, b, sem_in.at[i]) for i, (a, b) in enumerate(zip(ins, bufs))]
+    writes = [pltpu.make_async_copy(b, o, sem_out.at[i]) for i, (b, o) in enumerate(zip(bufs, outs))]
+    for c in reads:
+        c.start()
+    for r, w in zip(reads, writes):
+        r.wait()
+        w.start()
+    for w in writes:
+        w.wait()
+
+
+def handed_out(arrays):
+    hbm = pl.BlockSpec(memory_space=pltpu.HBM)
+    return pl.pallas_call(
+        copy_kernel,
+        out_shape=tuple(jax.ShapeDtypeStruct(a.shape, a.dtype) for a in arrays),
+        in_specs=[hbm] * 8,
+        out_specs=tuple([hbm] * 8),
+        scratch_shapes=[VM(a.shape, a.dtype) for a in arrays]
+        + [pltpu.SemaphoreType.DMA((8,)), pltpu.SemaphoreType.DMA((8,))],
+    )(*arrays)
 
 
 def on_device(
@@ -483,38 +538,40 @@
     vmem = pl.BlockSpec(memory_space=pltpu.VMEM)
     dma = pltpu.SemaphoreType.DMA
     shape = jax.ShapeDtypeStruct
-    return pl.pallas_call(
+    grads = pl.pallas_call(
         kernel,
         out_shape=(
             shape(w_gate.shape, BF), shape(w_up.shape, BF), shape(w_down.shape, BF),
             shape((192, 128), BF), shape((64, 64), F32),
             shape((64, 192), BF), shape((64, 192), BF), shape((64, 192), BF),
         ),
-        in_specs=[hbm, hbm, vmem, vmem, hbm, hbm, hbm, hbm, hbm, hbm, vmem, hbm],
+        in_specs=[hbm] * 12,
         out_specs=(hbm, hbm, hbm, vmem, vmem, vmem, vmem, vmem),
         scratch_shapes=[
+            VM((2, 192), jnp.int32), VM((2, 192), F32), VM((3, 64), F32), VM((128, 256), F32), VM((256, 128), F32),
             VM((192, 128), BF), VM((192, 2048), BF), VM((256, 2048), BF), VM((128, 2048), BF),
             VM((64, 192), BF), VM((64, 192), BF), VM((64, 192), BF), VM((64, 2048), BF),
             VM((512, 192), BF), VM((32, 2, SLOT, 128), BF), VM((16, 32, 2, SLOT, 128), BF),
             VM((512, 256), BF), VM((512, 128), BF), VM((4, 4, 32, SLOT, 128), BF),
             VM((4, 2, 4, 4, SLOT, 128), BF), VM((4, 2, 4, 8, SLOT, 128), BF), VM((4, 4, 8, SLOT, 128), BF),
-            VM((4, 2, 4, SLOT, 128), BF), VM((4, 2, 8, SLOT, 128), BF), VM((32, SLOT, 128), BF),
+            VM((4, 3, 8, SLOT, 128), BF), VM((32, SLOT, 128), BF),
             VM((32, SLOT, 128), BF),
             VM((256, 2048), BF), VM((128, 2048), BF), VM((256, 512), BF), VM((128, 512), BF),
-            VM((16, 192, 128), BF), VM((192, 2048), BF),
+            VM((16, 64, 192), BF), VM((16, 64, 128), BF), VM((16, 64, 192), BF), VM((16, 64, 192), BF), VM((16, 32, 128), BF),
             VM((64, 256), F32), VM((64, 128), BF), VM((64, 128), BF), VM((64, 192), F32), VM((64, 192), BF),
             VM((64, 256), F32), VM((64, 128), F32), VM((64, 128), F32),
             VM((2, 16, 32, 128), BF), VM((16, 32, 128), BF), VM((16, 32, 128), BF), VM((16, 32, 128), BF),
             VM((32, 128), F32), VM((32, 128), F32),
-            dma((9,)), dma((3,)), dma((17,)), dma((5,)), dma((4, 15)), dma((4, 8)), dma, dma((2, 15)), dma((2,)),
-            dma((3,)),
+            dma((12,)), dma((3,)), dma((23,)), dma((9,)), dma((8, 15)), dma((4, 7)), dma, dma((3,)), dma((2,)),
+            dma((4,)),
         ],
         compiler_params=pltpu.CompilerParams(
             collective_id=0, has_side_effects=True, vmem_limit_bytes=56 * 1024 * 1024
         ),
     )(
-        moe_in, cotangent, routing.T, route_weight, w_gate, w_up, w_down, gate_b, gate_c, value_x, conv_taps.T, out_proj
+        moe_in, cotangent, routing.T, route_weight.T, w_gate, w_up, w_down, gate_b, gate_c, value_x, conv_taps, out_proj
     )
+    return handed_out(grads)
 
 
 def solution(mesh):

time: 118 us -> 96.2 us (0.82)
  Pallas kernels: 107 us -> 95.4 us
  local copies, waits for them, and re-layouts: 9.81 us -> 0 us
    pallas_call x1, Pallas kernels: 107 us -> 93.1 us  [on_device(): pl.pallas_call(kernel, out_shape=(shape(w_gate.shape, BF), shape(w_up.sha...]
    unnamed x26 -> x0, local copies, waits for them, and re-layouts: 9.81 us -> none
    pallas_call x0 -> x1, Pallas kernels: none -> 2.36 us  [handed_out(): pl.pallas_call(copy_kernel, out_shape=tuple((jax.ShapeDtypeStruct(a.shape...]
where the time goes in v2:
time: 96.2 us; the launch traced here: 96.1 us
  Pallas kernels  95.4 us (99%)
    pallas_call x1, Pallas kernels, on_device(): pl.pallas_call(kernel, out_shape=(shape(w_gate.shape, BF), shape(w_up.sha...  93.1 us
    pallas_call x1, Pallas kernels, handed_out(): pl.pallas_call(copy_kernel, out_shape=tuple((jax.ShapeDtypeStruct(a.shape...  2.36 us

profile of v2, /device:TPU:1, one launch (start us, length us, event | category | flops | bytes accessed | tf_op | source)
XLA Modules:
  0.0 96.1 jit_solution(3538556061227068307)
XLA Ops:
  0.6 93.1 %shard_map.179 = (bf16[1,128,2048]{2,1,0:T(8,128)(2,1)}, bf16[1,128,2048]{2,1,0:T(8,128)(2,1)}, bf16[1,128,2048]{2,1,0:T(8,128)(2,1)}, bf16[192,128]{1,0:T(8,128...) custom-call(bf16[192,2048]{1,0:T(8,128)(2,1)} %moe_h.1, ...), custom_call_target="tpu_custom_call" | custom-call | tf_op jit(solution)/shard_map/pallas_call | solution.py:541
  93.7 2.4 %shard_map.180 = (bf16[1,128,2048]{2,1,0:T(8,128)(2,1)}, bf16[1,128,2048]{2,1,0:T(8,128)(2,1)}, bf16[1,128,2048]{2,1,0:T(8,128)(2,1)}, bf16[192,128]{1,0:T(8,128...) custom-call(bf16[1,128,2048]{2,1,0:T(8,128)(2,1)} %get-tuple-element.16., ...), custom_call_target="tpu_custom_call" | custom-call | tf_op jit(solution)/shard_map/pallas_call | solution.py:524

commit v3 on v2

--- a/solution.py
+++ b/solution.py
@@ -34,11 +34,11 @@
     moe_h, cot_h, route_h, weight_h, wg_h, wu_h, wd_h, gb_h, gc_h, vx_h, taps_h, op_h,
     o_wg, o_wu, o_wd, o_moe, o_proj, o_gb, o_gc, o_vx,
     route_t, weight_v, taps_v, table, turned, moe_v, cot_v, wgu, wdn, gb, gc, vx, op,
-    onehot, send, arr, gg, hd, part, r1, r2, zb, t1, fin, ret,
-    wgu_o, wdn_o, ggt, hdt, mixall, opt, ab, ar, qx,
+    onehot, send, arr, gg, hd, part, r1, r2, r3, zb, t1, fin, ret,
+    ggt, hdt, mixall, opt, ab, ar, qx,
     mixed, mx_tile, mx_halo, conv, act, cg, cg_tile, cg_halo,
     qb, qp, qs, qr, ts, tp_buf,
-    in_sem, out_sem, snd, z1_sem, ag_sem, rs_sem, ret_sem, w_sem, hl_sem, q_sem,
+    in_sem, snd, z1_sem, ag_sem, rs_sem, ret_sem, w_sem, hl_sem, q_sem,
 ):
     sp = lax.axis_index("sp")
     tp = lax.axis_index("tp")
@@ -164,8 +164,12 @@
                 z1_sem.at[8 if o == 0 else j // 2], (e, tp),
             )
 
-    for o in order:
-        dispatch_to(o)
+    def dispatch(*chunks):
+        for o in order:
+            if PLACE[(-o) % 16] % 8 // 2 in chunks:
+                dispatch_to(o)
+
+    dispatch(0, 1)
     after = (lax.rem(sp + 1, 32), tp)
     ahead = (lax.rem(sp + 31, 32), tp)
     push(mx_tile, mx_halo, 1, hl_sem.at[0], after)
@@ -177,7 +181,7 @@
             a = 2
         landed(arr.at[tp, a : 4 * i + 4, :, 0:CAP], z1_sem.at[i])
 
-    def gather_steps(region, dims, group, sem):
+    def gather_steps(region, dims, group, sem, direct):
         d1, d2 = dims
 
         def lane(a, b):
@@ -202,6 +206,8 @@
             own = region(lane(0, 0))
             for s in (1, -1):
                 push(own, own, group, sem1(s), near(d1, s))
+            if direct:
+                push(own, own, group, sem(2), near(d1, 2))
             for s in (1, -1):
                 push(own, own, group, sem2(0, s), near(d2, s))
 
@@ -219,8 +225,9 @@
         def e1():
             for s in (1, -1):
                 landed(region(lane(-s, 0)), sem1(s))
-                block = region(lane(-s, 0), half(s))
-                push(block, block, group, sem(2), near(d1, s))
+                if not direct:
+                    block = region(lane(-s, 0), half(s))
+                    push(block, block, group, sem(2), near(d1, s))
             for s in (1, -1):
                 across(-s)
             on(0)
@@ -228,10 +235,10 @@
         def e2():
             landed(region(lane(2, 0)), sem(2))
             across(2)
+
+        def e3():
             on(1)
             on(-1)
-
-        def e3():
             on(2)
 
         def e4():
@@ -249,29 +256,40 @@
 
     dims_of = (("x", "y"), ("x", "y"), ("y", "x"), ("y", "x"))
     ag = [
-        gather_steps(rows_of(i), dims_of[i // 2], 2 + i, functools.partial(lambda i, k: ag_sem.at[i, k], i))
+        gather_steps(rows_of(i), dims_of[i // 2], 2 + i, functools.partial(lambda i, k: ag_sem.at[i, k], i), True)
         for i in range(8)
     ]
 
-    def expert_rows(q):
-        a = 8 * q
-        xm = jnp.concatenate([arr[l, a : a + 8, 0].reshape(128, 128) for l in range(16)], axis=1)
-        pre = nt(xm, wgu[...])
-        xc = jnp.concatenate([arr[l, a : a + 8, 1].reshape(128, 128) for l in range(16)], axis=1)
-        hg = nt(xc, wdn[...])
+    def expert_rows(c):
+        parts = (4 * c, 4 * c + 16)
+
+        def wide(kind):
+            return jnp.concatenate(
+                [
+                    jnp.concatenate([arr[l, a : a + 4, kind].reshape(64, 128) for a in parts], axis=0)
+                    for l in range(16)
+                ],
+                axis=1,
+            )
+
+        pre = nt(wide(0), wgu[...])
+        hg = nt(wide(1), wdn[...])
         gate, up = pre[:, 0:128], pre[:, 128:256]
         sig = jax.nn.sigmoid(gate)
         silu = gate * sig
-        rows = slice(128 * q, 128 * q + 128)
-        hd[rows, :] = (silu * up).astype(BF)
-        gg[rows, 0:128] = (hg * up * sig * (1.0 + gate * (1.0 - sig))).astype(BF)
-        gg[rows, 128:256] = (hg * silu).astype(BF)
-        g = gg[rows, :]
+        hidden = (silu * up).astype(BF)
+        g = jnp.concatenate([hg * up * sig * (1.0 + gate * (1.0 - sig)), hg * silu], axis=1).astype(BF)
+        for h, a in enumerate(parts):
+            hd[16 * a : 16 * a + 64, :] = hidden[64 * h : 64 * h + 64]
+            gg[16 * a : 16 * a + 64, :] = g[64 * h : 64 * h + 64]
         for i in range(8):
             pv = nn(g, wgu[:, 256 * i : 256 * i + 256]).astype(BF)
             for k in (0, 1):
                 l = 2 * i + k
-                part[l // 4, l % 4, a : a + 8] = pv[:, 128 * k : 128 * k + 128].reshape(8, SLOT, 128)
+                for h, a in enumerate(parts):
+                    part[l // 4, l % 4, a : a + 4] = pv[
+                        64 * h : 64 * h + 64, 128 * k : 128 * k + 128
+                    ].reshape(4, SLOT, 128)
 
     def back(owner):
         return lax.rem(sp - owner + 32, 32)
@@ -279,12 +297,12 @@
     def scatter_steps(q, dims):
         d1, d2 = dims
         at = {"x": x, "y": y}
-        a = 8 * q
+        a = 4 * q
 
         def half(s):
-            return (0, 4) if s == 1 else (4, 4)
-
-        def bundle(d, lo=0, n=8):
+            return (0, 2) if s == 1 else (2, 2)
+
+        def bundle(d, lo=0, n=4):
             i = lax.rem(at[d1] + d + 4, 4)
             if d1 == "y":
                 return part.at[i, :, a + lo : a + lo + n]
@@ -299,11 +317,20 @@
         def sem(i):
             return rs_sem.at[q, i]
 
+        direct = q % 4 == 3
+
         def q1():
+            if direct:
+                push(cut(bundle(2)), cut(r3.at[q // 4]), 10 + q, sem(0), near(d1, 2))
+                for s in (1, -1):
+                    push(cut(bundle(s)), cut(r2.at[q, w(s)]), 10 + q, sem(2 + w(s)), near(d1, s))
+                return
             for s in (1, -1):
                 push(cut(bundle(2, *half(s))), cut(r1.at[q, w(s)]), 10 + q, sem(w(s)), near(d1, s))
 
         def q2():
+            if direct:
+                return
             for s in (1, -1):
                 landed(cut(r1.at[q, w(s)]), sem(w(s)))
                 mine = bundle(s, *half(s))
@@ -313,7 +340,11 @@
         def q3():
             for s in (1, -1):
                 landed(cut(r2.at[q, w(s)]), sem(2 + w(s)))
-            zb[q] = (bundle(0)[...].astype(F32) + r2[q, 0].astype(F32) + r2[q, 1].astype(F32)).astype(BF)
+            own = bundle(0)[...].astype(F32)
+            if direct:
+                landed(cut(r3.at[q // 4]), sem(0))
+                own = own + r3[q // 4].astype(F32)
+            zb[q] = (own + r2[q, 0].astype(F32) + r2[q, 1].astype(F32)).astype(BF)
             for k, s in enumerate((2, 1, -1)):
                 i = lax.rem(at[d2] + s + 4, 4)
                 push(cut(zb.at[q, i], 3), cut(t1.at[q, k], 3), 10 + q, sem(4 + k), near(d2, s))
@@ -321,78 +352,86 @@
         def q4():
             for k in range(3):
                 landed(cut(t1.at[q, k], 3), sem(4 + k))
-            fin[a : a + 8] = (
+            fin[a : a + 4] = (
                 zb[q, at[d2]].astype(F32) + t1[q, 0].astype(F32) + t1[q, 1].astype(F32) + t1[q, 2].astype(F32)
             ).astype(BF)
-            for j in range(4 * q + 3, 4 * q - 1, -1):
+            for j in (2 * q + 1, 2 * q):
                 for cc in (0, 1):
                     if OFFSETS[j] == 0:
                         if cc == 0:
-                            push(fin.at[1 - core, 0:CAP], ret.at[back(partner[0]), 0:CAP], 14, ret_sem, partner)
+                            push(fin.at[1 - core, 0:CAP], ret.at[back(partner[0]), 0:CAP], 18, ret_sem, partner)
                             ret[0, 0:CAP] = fin[core, 0:CAP]
                     else:
                         dev = (lax.rem(z + OFFSETS[j] + 16, 16) * 2 + cc, tp)
-                        push(fin.at[2 * j + cc, 0:CAP], ret.at[back(dev[0]), 0:CAP], 14, ret_sem, dev)
+                        push(fin.at[2 * j + cc, 0:CAP], ret.at[back(dev[0]), 0:CAP], 18, ret_sem, dev)
 
         return q1, q2, q3, q4
 
-    rs = [scatter_steps(q, dims_of[q][::-1]) for q in range(4)]
+    rs = [scatter_steps(i, dims_of[i // 2][::-1]) for i in range(8)]
 
     def both(steps, c, k):
         steps[c][k]()
         steps[c + len(steps) // 2][k]()
 
-    z_arrived(0)
-    z_arrived(4)
-    both(ag, 0, 0)
-    z_arrived(1)
-    z_arrived(5)
-    both(ag, 1, 0)
-    both(ag, 0, 1)
-    z_arrived(2)
-    z_arrived(6)
-    both(ag, 2, 0)
-    loads[4].wait()
-    landed(mx_halo, hl_sem.at[0])
     lane_id = lax.broadcasted_iota(jnp.int32, (64, 128), 1)
-    halo = jnp.where(sp == 0, 0.0, mx_halo[...].astype(F32))
-    mixed[:, 128:256] = jnp.where(lane_id < 64, mixed[:, 128:256], halo)
-    m = mixed[...]
-    conv[...] = (
-        taps[2] * m + taps[1] * pltpu.roll(m, 1, 1) + taps[0] * pltpu.roll(m, 2, 1)
-    )[:, 0:192]
-    act[...] = (gb[...].astype(F32) * conv[...]).astype(BF)
-    for c in loads[5:9]:
-        c.wait()
-    both(ag, 1, 1)
-    z_arrived(3)
-    z_arrived(7)
-    both(ag, 3, 0)
-    both(ag, 0, 2)
-    both(ag, 2, 1)
-    both(ag, 1, 2)
-    both(ag, 3, 1)
-    both(ag, 0, 3)
-    both(ag, 2, 2)
-    both(ag, 1, 3)
-    both(ag, 0, 4)
-    both(ag, 3, 2)
-    both(ag, 2, 3)
-    both(ag, 1, 4)
-    both(ag, 3, 3)
-    expert_rows(0)
-    expert_rows(2)
-    both(rs, 0, 0)
-    both(ag, 2, 4)
-    both(ag, 3, 4)
-    expert_rows(1)
-    expert_rows(3)
-    both(rs, 1, 0)
-    both(rs, 0, 1)
-    both(rs, 1, 1)
-    both(rs, 0, 2)
-    both(rs, 1, 2)
-    both(rs, 0, 3)
+
+    def start(i):
+        z_arrived(i)
+        ag[i][0]()
+        if i == 0:
+            dispatch(2, 3)
+
+    def step(steps, i, k):
+        steps[i][k]()
+
+    def forward():
+        loads[4].wait()
+        landed(mx_halo, hl_sem.at[0])
+        halo = jnp.where(sp == 0, 0.0, mx_halo[...].astype(F32))
+        mixed[:, 128:256] = jnp.where(lane_id < 64, mixed[:, 128:256], halo)
+        m = mixed[...]
+        conv[...] = (
+            taps[2] * m + taps[1] * pltpu.roll(m, 1, 1) + taps[0] * pltpu.roll(m, 2, 1)
+        )[:, 0:192]
+        act[...] = (gb[...].astype(F32) * conv[...]).astype(BF)
+        for c in loads[5:9]:
+            c.wait()
+
+    def rows(c):
+        both(ag, c, 4)
+        expert_rows(c)
+        both(rs, c, 0)
+
+    plane = sorted(
+        ((dy, dx) for dy in range(4) for dx in range(4) if (dy, dx) != (0, 0)),
+        key=lambda d: -(min(d[0], 4 - d[0]) + min(d[1], 4 - d[1])),
+    )
+
+    def lanes():
+        for dy, dx in plane:
+            lane = lax.rem(y + dy, 4) * 4 + lax.rem(x + dx, 4)
+            yield lane, lax.rem(lane - tp + 16, 16)
+
+    def exchange():
+        mixall[0] = act[...]
+        opt[0] = op[:, col]
+        for lane, b in lanes():
+            push(act, mixall.at[16 - b], 19, w_sem.at[0], (sp, lane))
+        for lane, b in lanes():
+            there = pl.ds(pl.multiple_of(lane * 128, 128), 128)
+            push(op.at[:, there], opt.at[16 - b], 20, w_sem.at[1], (sp, lane))
+
+    due = [(17.3, forward), (46.0, exchange)]
+    for i, t in enumerate((10.7, 13.5, 16.5, 20.0, 12.0, 15.0, 17.5, 20.8)):
+        due.append((t, functools.partial(start, i)))
+        for k, dt in ((1, 4.2), (2, 4.8), (3, 9.0)):
+            due.append((t + dt, functools.partial(step, ag, i, k)))
+    for c, t in enumerate((26.5, 29.5, 32.0, 33.5)):
+        due.append((t, functools.partial(rows, c)))
+        for k, dt in ((1, 3.7), (2, 7.4), (3, 11.1)):
+            due.append((t + dt + 1.8 * (c == 3), functools.partial(both, rs, c, k)))
+    for _, event in sorted(due, key=lambda e: e[0]):
+        event()
 
     ggt[...] = gg[...].astype(F32).T.astype(BF)
     hdt[...] = hd[...].astype(F32).T.astype(BF)
@@ -400,31 +439,14 @@
     def weight_grads(i, carry):
         out = pl.ds(pl.multiple_of(i * 256, 256), 256)
         xm = jnp.concatenate([arr[2 * i, :, 0].reshape(512, 128), arr[2 * i + 1, :, 0].reshape(512, 128)], axis=1)
-        wgu_o[:, out] = nn(ggt[...], xm).astype(BF)
+        both_grads = nn(ggt[...], xm).astype(BF)
+        o_wg[0, :, out] = both_grads[0:128]
+        o_wu[0, :, out] = both_grads[128:256]
         xc = jnp.concatenate([arr[2 * i, :, 1].reshape(512, 128), arr[2 * i + 1, :, 1].reshape(512, 128)], axis=1)
-        wdn_o[:, out] = nn(hdt[...], xc).astype(BF)
+        o_wd[0, :, out] = nn(hdt[...], xc).astype(BF)
         return carry
 
-    both(rs, 1, 3)
-
-    mixall[0] = act[...]
-    opt[0] = op[:, col]
-    for b in range(1, 16):
-        lane = lax.rem(tp + b, 16)
-        push(act, mixall.at[16 - b], 15, w_sem.at[0], (sp, lane))
-    for b in range(1, 16):
-        lane = lax.rem(tp + b, 16)
-        there = pl.ds(pl.multiple_of(lane * 128, 128), 128)
-        push(op.at[:, there], opt.at[16 - b], 16, w_sem.at[1], (sp, lane))
     lax.fori_loop(0, 8, weight_grads, 0)
-    stores = [
-        pltpu.make_async_copy(wgu_o.at[0:128], o_wg.at[0], out_sem.at[0]),
-        pltpu.make_async_copy(wgu_o.at[128:256], o_wu.at[0], out_sem.at[1]),
-        pltpu.make_async_copy(wdn_o, o_wd.at[0], out_sem.at[2]),
-    ]
-    for c in stores:
-        c.start()
-
     landed(ret.at[1:32, 0:CAP], ret_sem)
     mine = tn(onehot[...], ret[...].reshape(32 * SLOT, 128)).astype(BF)
     o_moe[...] = mine
@@ -435,7 +457,7 @@
         pq = nn(mixall[4 * i : 4 * i + 4].reshape(256, 192), stream).astype(BF).reshape(4, 2, 32, 128)
         for h in (0, 1):
             qb[h, 4 * i : 4 * i + 4] = pq[:, h]
-    push(qb.at[1 - core], qp, 17, q_sem.at[0], partner)
+    push(qb.at[1 - core], qp, 21, q_sem.at[0], partner)
     landed(opt.at[1:16], w_sem.at[1])
     for i in range(4):
         pa = nt(opt[4 * i : 4 * i + 4].reshape(256, 128), stream).astype(BF)
@@ -443,15 +465,15 @@
     landed(qp, q_sem.at[0])
     qs[...] = (qb[core].astype(F32) + qp[...].astype(F32)).astype(BF)
     qx[0] = qs[0]
-    for b in range(1, 16):
-        push(qs.at[b], qx.at[16 - b], 18, q_sem.at[3], (sp, lax.rem(tp + b, 16)))
-    for b in range(1, 16):
-        push(ab.at[b], ar.at[16 - b], 19, w_sem.at[2], (sp, lax.rem(tp + b, 16)))
+    for lane, b in lanes():
+        push(qs.at[b], qx.at[16 - b], 22, q_sem.at[3], (sp, lane))
+    for lane, b in lanes():
+        push(ab.at[b], ar.at[16 - b], 23, w_sem.at[2], (sp, lane))
     landed(qx.at[1:16], q_sem.at[3])
     for o in order[:0:-1]:
         zz = lax.rem(z + o + 16, 16)
         push(
-            qx.at[lax.rem(zz - tp + 16, 16)], qr.at[PLACE[(-o) % 16]], 20, q_sem.at[1], (zz * 2 + core, tp)
+            qx.at[lax.rem(zz - tp + 16, 16)], qr.at[PLACE[(-o) % 16]], 24, q_sem.at[1], (zz * 2 + core, tp)
         )
     landed(ar.at[1:16], w_sem.at[2])
     act_grad = ab[0].astype(F32)
@@ -462,7 +484,7 @@
     cg[...] = jnp.zeros(cg.shape, F32)
     cg[:, 0:192] = act_grad * gb[...].astype(F32)
     cg_tile[...] = pltpu.roll(cg[:, 0:128], 64, 1)
-    push(cg_tile, cg_halo, 21, hl_sem.at[1], ahead)
+    push(cg_tile, cg_halo, 25, hl_sem.at[1], ahead)
     landed(cg_halo, hl_sem.at[1])
     later = jnp.where(sp == 31, 0.0, cg_halo[...])
     cg[:, 128:256] = jnp.where(lane_id < 64, cg[:, 128:256], later)
@@ -478,7 +500,7 @@
     for o in order[1:]:
         total = total + qr[PLACE[o % 16]].astype(F32)
     ts[...] = total
-    push(ts, tp_buf, 22, q_sem.at[2], partner)
+    push(ts, tp_buf, 26, q_sem.at[2], partner)
     landed(tp_buf, q_sem.at[2])
     low = jnp.where(core == 0, ts[...], tp_buf[...])
     high = jnp.where(core == 0, tp_buf[...], ts[...])
@@ -490,44 +512,35 @@
     left(mx_tile, 1)
     for i in range(8):
         left(arr.at[0:15, 4 * i : 4 * i + 4, :, 0:CAP], 2 + i)
-    for q in range(4):
-        left(arr.at[0:15, 8 * q : 8 * q + 8, 0, 0:CAP], 10 + q)
-    left(ret.at[1:32, 0:CAP], 14)
-    left(mixall.at[1:16], 15)
-    left(opt.at[1:16], 16)
-    left(qp, 17)
-    left(qx.at[1:16], 18)
-    left(ar.at[1:16], 19)
-    left(qr.at[1:16], 20)
-    left(cg_tile, 21)
-    left(ts, 22)
-    for c in stores:
+        left(arr.at[0:15, 4 * i : 4 * i + 4, 0, 0:CAP], 10 + i)
+    left(ret.at[1:32, 0:CAP], 18)
+    left(mixall.at[1:16], 19)
+    left(opt.at[1:16], 20)
+    left(qp, 21)
+    left(qx.at[1:16], 22)
+    left(ar.at[1:16], 23)
+    left(qr.at[1:16], 24)
+    left(cg_tile, 25)
+    left(ts, 26)
+
+
+def copy_kernel(*refs):
+    ins, outs, sem = refs[:8], refs[8:16], refs[16]
+    copies = [pltpu.make_async_copy(a, o, sem.at[i]) for i, (a, o) in enumerate(zip(ins, outs))]
+    for c in copies:
+        c.start()
+    for c in copies:
         c.wait()
 
 
-def copy_kernel(*refs):
-    ins, outs, rest = refs[:8], refs[8:16], refs[16:]
-    bufs, sem_in, sem_out = rest[:8], rest[8], rest[9]
-    reads = [pltpu.make_async_copy(a, b, sem_in.at[i]) for i, (a, b) in enumerate(zip(ins, bufs))]
-    writes = [pltpu.make_async_copy(b, o, sem_out.at[i]) for i, (b, o) in enumerate(zip(bufs, outs))]
-    for c in reads:
-        c.start()
-    for r, w in zip(reads, writes):
-        r.wait()
-        w.start()
-    for w in writes:
-        w.wait()
-
-
 def handed_out(arrays):
-    hbm = pl.BlockSpec(memory_space=pltpu.HBM)
     return pl.pallas_call(
         copy_kernel,
         out_shape=tuple(jax.ShapeDtypeStruct(a.shape, a.dtype) for a in arrays),
-        in_specs=[hbm] * 8,
-        out_specs=tuple([hbm] * 8),
-        scratch_shapes=[VM(a.shape, a.dtype) for a in arrays]
-        + [pltpu.SemaphoreType.DMA((8,)), pltpu.SemaphoreType.DMA((8,))],
+        in_specs=[pl.BlockSpec(memory_space=pltpu.VMEM)] * 8,
+        out_specs=tuple([pl.BlockSpec(memory_space=pltpu.HBM)] * 8),
+        scratch_shapes=[pltpu.SemaphoreType.DMA((8,))],
+        compiler_params=pltpu.CompilerParams(vmem_limit_bytes=8 * 1024 * 1024),
     )(*arrays)
 
 
@@ -537,36 +550,34 @@
     hbm = pl.BlockSpec(memory_space=pltpu.HBM)
     vmem = pl.BlockSpec(memory_space=pltpu.VMEM)
     dma = pltpu.SemaphoreType.DMA
-    shape = jax.ShapeDtypeStruct
     grads = pl.pallas_call(
         kernel,
         out_shape=(
-            shape(w_gate.shape, BF), shape(w_up.shape, BF), shape(w_down.shape, BF),
-            shape((192, 128), BF), shape((64, 64), F32),
-            shape((64, 192), BF), shape((64, 192), BF), shape((64, 192), BF),
+            VM(w_gate.shape, BF), VM(w_up.shape, BF), VM(w_down.shape, BF), VM((192, 128), BF), VM((64, 64), F32),
+            VM((64, 192), BF), VM((64, 192), BF), VM((64, 192), BF),
         ),
         in_specs=[hbm] * 12,
-        out_specs=(hbm, hbm, hbm, vmem, vmem, vmem, vmem, vmem),
+        out_specs=tuple([vmem] * 8),
         scratch_shapes=[
             VM((2, 192), jnp.int32), VM((2, 192), F32), VM((3, 64), F32), VM((128, 256), F32), VM((256, 128), F32),
             VM((192, 128), BF), VM((192, 2048), BF), VM((256, 2048), BF), VM((128, 2048), BF),
             VM((64, 192), BF), VM((64, 192), BF), VM((64, 192), BF), VM((64, 2048), BF),
             VM((512, 192), BF), VM((32, 2, SLOT, 128), BF), VM((16, 32, 2, SLOT, 128), BF),
             VM((512, 256), BF), VM((512, 128), BF), VM((4, 4, 32, SLOT, 128), BF),
-            VM((4, 2, 4, 4, SLOT, 128), BF), VM((4, 2, 4, 8, SLOT, 128), BF), VM((4, 4, 8, SLOT, 128), BF),
-            VM((4, 3, 8, SLOT, 128), BF), VM((32, SLOT, 128), BF),
+            VM((8, 2, 4, 2, SLOT, 128), BF), VM((8, 2, 4, 4, SLOT, 128), BF), VM((2, 4, 4, SLOT, 128), BF), VM((8, 4, 4, SLOT, 128), BF),
+            VM((8, 3, 4, SLOT, 128), BF), VM((32, SLOT, 128), BF),
             VM((32, SLOT, 128), BF),
-            VM((256, 2048), BF), VM((128, 2048), BF), VM((256, 512), BF), VM((128, 512), BF),
+            VM((256, 512), BF), VM((128, 512), BF),
             VM((16, 64, 192), BF), VM((16, 64, 128), BF), VM((16, 64, 192), BF), VM((16, 64, 192), BF), VM((16, 32, 128), BF),
             VM((64, 256), F32), VM((64, 128), BF), VM((64, 128), BF), VM((64, 192), F32), VM((64, 192), BF),
             VM((64, 256), F32), VM((64, 128), F32), VM((64, 128), F32),
             VM((2, 16, 32, 128), BF), VM((16, 32, 128), BF), VM((16, 32, 128), BF), VM((16, 32, 128), BF),
             VM((32, 128), F32), VM((32, 128), F32),
-            dma((12,)), dma((3,)), dma((23,)), dma((9,)), dma((8, 15)), dma((4, 7)), dma, dma((3,)), dma((2,)),
+            dma((12,)), dma((27,)), dma((9,)), dma((8, 15)), dma((8, 7)), dma, dma((3,)), dma((2,)),
             dma((4,)),
         ],
         compiler_params=pltpu.CompilerParams(
-            collective_id=0, has_side_effects=True, vmem_limit_bytes=56 * 1024 * 1024
+            collective_id=0, has_side_effects=True, vmem_limit_bytes=60 * 1024 * 1024
         ),
     )(
         moe_in, cotangent, routing.T, route_weight.T, w_gate, w_up, w_down, gate_b, gate_c, value_x, conv_taps, out_proj

time: 96.2 us -> 87.4 us (0.909)
  Pallas kernels: 95.4 us -> 86.6 us
    pallas_call x1, Pallas kernels: 93.1 us -> 85.3 us  [on_device(): pl.pallas_call(kernel, out_shape=(VM(w_gate.shape, BF), VM(w_up.shape, BF...]
    pallas_call x1, Pallas kernels: 2.36 us -> 1.26 us  [handed_out(): pl.pallas_call(copy_kernel, out_shape=tuple((jax.ShapeDtypeStruct(a.shape...]
where the time goes in v3:
time: 87.4 us; the launch traced here: 87.2 us
  Pallas kernels  86.6 us (99%)
    pallas_call x1, Pallas kernels, on_device(): pl.pallas_call(kernel, out_shape=(VM(w_gate.shape, BF), VM(w_up.shape, BF...  85.3 us

profile of v3, /device:TPU:1, one launch (start us, length us, event | category | flops | bytes accessed | tf_op | source)
XLA Modules:
  0.0 87.2 jit_solution(16312583633978732986)
XLA Ops:
  0.6 85.3 %shard_map.179 = (bf16[1,128,2048]{2,1,0:T(8,128)(2,1)S(1)}, bf16[1,128,2048]{2,1,0:T(8,128)(2,1)S(1)}, bf16[1,128,2048]{2,1,0:T(8,128)(2,1)S(1)}, bf16[192,128]...) custom-call(bf16[192,2048]{1,0:T(8,128)(2,1)} %moe_h.1, ...), custom_call_target="tpu_custom_call" | custom-call | tf_op jit(solution)/shard_map/pallas_call | solution.py:553
  86.0 1.3 %shard_map.180 = (bf16[1,128,2048]{2,1,0:T(8,128)(2,1)}, bf16[1,128,2048]{2,1,0:T(8,128)(2,1)}, bf16[1,128,2048]{2,1,0:T(8,128)(2,1)}, bf16[192,128]{1,0:T(8,128...) custom-call(bf16[1,128,2048]{2,1,0:T(8,128)(2,1)S(1)} %get-tuple-element, ...), custom_call_target="tpu_custom_call" | custom-call | tf_op jit(solution)/shard_map/pallas_call | solution.py:537

commit v4 on v3

--- a/solution.py
+++ b/solution.py
@@ -38,7 +38,7 @@
     ggt, hdt, mixall, opt, ab, ar, qx,
     mixed, mx_tile, mx_halo, conv, act, cg, cg_tile, cg_halo,
     qb, qp, qs, qr, ts, tp_buf,
-    in_sem, snd, z1_sem, ag_sem, rs_sem, ret_sem, w_sem, hl_sem, q_sem,
+    in_sem, snd, z1_sem, ag_sem, rs_sem, ret_sem, w_sem, hl_sem, q_sem, tok,
 ):
     sp = lax.axis_index("sp")
     tp = lax.axis_index("tp")
@@ -53,7 +53,7 @@
 
     barrier = pltpu.get_barrier_semaphore()
     order = (0, 1, -1, 2, -2, 3, -3, 4, -4, 5, -5, 6, -6, 7, -7, 8)
-    for o in order[::-1]:
+    for o in order[8::-1]:
         zz = lax.rem(z + o + 16, 16)
         for cc in (0, 1):
             if o == 0:
@@ -148,7 +148,12 @@
     mx_tile[...] = pltpu.roll(mixed[:, 128:256], 64, 1).astype(BF)
 
     arr[tp, core, :, 0:CAP] = send[0, :, 0:CAP]
-    pl.semaphore_wait(barrier, 46)
+    pl.semaphore_wait(barrier, 32)
+
+    for way, o in ((0, -4), (1, 4)):
+        pl.semaphore_signal(
+            tok.at[way], inc=1, device_id=(lax.rem(z + o + 16, 16) * 2 + core, tp), device_id_type=MESH
+        )
 
     def dispatch_to(o):
         j = PLACE[(-o) % 16]
@@ -379,6 +384,8 @@
         z_arrived(i)
         ag[i][0]()
         if i == 0:
+            for way in (0, 1):
+                pl.semaphore_wait(tok.at[way], 1)
             dispatch(2, 3)
 
     def step(steps, i, k):
@@ -428,8 +435,9 @@
             due.append((t + dt, functools.partial(step, ag, i, k)))
     for c, t in enumerate((26.5, 29.5, 32.0, 33.5)):
         due.append((t, functools.partial(rows, c)))
-        for k, dt in ((1, 3.7), (2, 7.4), (3, 11.1)):
-            due.append((t + dt + 1.8 * (c == 3), functools.partial(both, rs, c, k)))
+        last = 43.0 + 0.2 * c if c < 3 else 46.4
+        for k, u in ((1, t + 3.7), (2, 42.7 if c == 3 else t + 7.4), (3, last)):
+            due.append((u, functools.partial(both, rs, c, k)))
     for _, event in sorted(due, key=lambda e: e[0]):
         event()
 
@@ -574,7 +582,7 @@
             VM((2, 16, 32, 128), BF), VM((16, 32, 128), BF), VM((16, 32, 128), BF), VM((16, 32, 128), BF),
             VM((32, 128), F32), VM((32, 128), F32),
             dma((12,)), dma((27,)), dma((9,)), dma((8, 15)), dma((8, 7)), dma, dma((3,)), dma((2,)),
-            dma((4,)),
+            dma((4,)), pltpu.SemaphoreType.REGULAR((2,)),
         ],
         compiler_params=pltpu.CompilerParams(
             collective_id=0, has_side_effects=True, vmem_limit_bytes=60 * 1024 * 1024

time: 87.4 us -> 86.5 us (0.990)
  Pallas kernels: 86.6 us -> 85.7 us
where the time goes in v4:
time: 86.5 us; the launch traced here: 86.4 us
  Pallas kernels  85.7 us (99%)
    pallas_call x1, Pallas kernels, on_device(): pl.pallas_call(kernel, out_shape=(VM(w_gate.shape, BF), VM(w_up.shape, BF...  84.5 us

profile of v4, /device:TPU:1, one launch (start us, length us, event | category | flops | bytes accessed | tf_op | source)
XLA Modules:
  0.0 86.4 jit_solution(1419286218507677648)
XLA Ops:
  0.6 84.5 %shard_map.179 = (bf16[1,128,2048]{2,1,0:T(8,128)(2,1)S(1)}, bf16[1,128,2048]{2,1,0:T(8,128)(2,1)S(1)}, bf16[1,128,2048]{2,1,0:T(8,128)(2,1)S(1)}, bf16[192,128]...) custom-call(bf16[192,2048]{1,0:T(8,128)(2,1)} %moe_h.1, ...), custom_call_target="tpu_custom_call" | custom-call | tf_op jit(solution)/shard_map/pallas_call | solution.py:561
  85.1 1.3 %shard_map.180 = (bf16[1,128,2048]{2,1,0:T(8,128)(2,1)}, bf16[1,128,2048]{2,1,0:T(8,128)(2,1)}, bf16[1,128,2048]{2,1,0:T(8,128)(2,1)}, bf16[192,128]{1,0:T(8,128...) custom-call(bf16[1,128,2048]{2,1,0:T(8,128)(2,1)S(1)} %get-tuple-element, ...), custom_call_target="tpu_custom_call" | custom-call | tf_op jit(solution)/shard_map/pallas_call | solution.py:545
